TPU v7x, 128 devices: a whole 4x4x4 slice. The times are simulated.
128 devices in a mesh: dp: 4 (over x), kv: 16 (over z, y), tp: 2 (over core).
Axes of the slice: x: 4, y: 4, z: 4, core: 2. Of those that a mesh axis runs over, the one named last changes fastest.
Arguments:
- pieces: bfloat16 [4096, 8, 2048], P(('kv', 'tp'), 'dp'), parts along dimension 1, may hold values from -6 to 6
- new_tokens: bfloat16 [256, 2048], P(('dp', 'kv', 'tp')), parts along dimension 0, may hold values from -6 to 6
- w_query: bfloat16 [2048, 1024], P(None, 'tp'), may hold values from -0.125 to 0.125
- w_key: bfloat16 [2048, 1024], P(None, 'tp'), may hold values from -0.125 to 0.125
- w_value: bfloat16 [2048, 2048], P(None, 'tp'), may hold values from -0.125 to 0.125
- w_decay: bfloat16 [2048, 1024], P(None, 'tp'), may hold values from -0.125 to 0.125
- decay_bias: float32 [1024], replicated, may hold values from 0 to 9
- norm_gain: float32 [2048], replicated, may hold values from 0.1 to 1.9
- head_gain: float32 [2048], replicated, may hold values from 0.1 to 1.9
- w_out: bfloat16 [2048, 2048], replicated, may hold values from -0.125 to 0.125
- prompt_state: float32 [8, 8, 128, 256], P('dp', 'tp', 'kv'), parts along dimension 0, may hold values from -8 to 8
- decode_state: float32 [256, 8, 128, 256], P(('dp', 'kv'), 'tp'), parts along dimension 0, may hold values from -8 to 8
Outputs:
- mixed_piece: bfloat16 [4096, 8, 2048], P(('kv', 'tp'), 'dp'), parts along dimension 1
- mixed_decode: bfloat16 [256, 2048], P(('dp', 'kv', 'tp')), parts along dimension 0
- prompt_state_out: float32 [8, 8, 128, 256], P('dp', 'tp', 'kv'), parts along dimension 0
- decode_state_out: float32 [256, 8, 128, 256], P(('dp', 'kv'), 'tp'), parts along dimension 0
There are 4 independent parts, one for each index of `dp`. A program takes and returns all parts, laid end to end along the dimension named above; an argument that names none is the same for every part. Nothing has to cross between parts.
All inputs are finite; a program needn't handle non-finite values.
Results may differ from a plain program's by a relative error of at most 0.014.
Values may be sent and summed in bfloat16 or wider, within the bound.
A program may use at most 128 MiB of HBM per device.

v0:
```python
import jax
import jax.numpy as jnp
from jax import lax
from jax.sharding import Mesh
from jax.sharding import PartitionSpec as P

DK = 128
DV = 256
BLOCK = 64
KV = ("kv_0", "kv_1")
KV_TP = ("kv_0", "kv_1", "tp")
DP_KV_TP = ("dp", "kv_0", "kv_1", "tp")
DP_KV = ("dp", "kv_0", "kv_1")


norm_eps = 0.1
decay_tau = 16.0
part_limit = 16


def copy_for_each(array, axis):
    copies = jnp.broadcast_to(array, (lax.axis_size(axis), *array.shape))
    return lax.all_to_all(copies, axis, split_axis=0, concat_axis=0, tiled=True)


def joined_along(pieces, dim):
    pieces = jnp.moveaxis(pieces, 0, dim)
    shape = pieces.shape
    return pieces.reshape(*shape[:dim], shape[dim] * shape[dim + 1], *shape[dim + 2 :])


def collect(array, axis, dim):
    pieces = copy_for_each(array, axis)
    return joined_along(pieces, dim)


def nothing_yet(array, identity):
    return jax.tree.map(
        lambda a, e: jnp.broadcast_to(jnp.asarray(e, a.dtype), a.shape), array, identity
    )


def entering(array, axes, combine, identity):
    before = start = nothing_yet(array, identity)
    subtotal = array
    for axis in reversed(axes):
        count, index = (lax.axis_size(axis), lax.axis_index(axis))
        pieces = jax.tree.map(lambda part: lax.all_gather(part, axis), subtotal)
        inside, subtotal = (start, start)
        for k in range(count):
            passed = k < index
            subtotal = combine(subtotal, jax.tree.map(lambda part: part[k], pieces))
            inside = jax.tree.map(lambda new, old: jnp.where(passed, new, old), subtotal, inside)
        before = combine(inside, before)
    return before


def cut_along(array, dim, count):
    shape = array.shape
    pieces = array.reshape(*shape[:dim], count, shape[dim] // count, *shape[dim + 1 :])
    return jnp.moveaxis(pieces, dim, 0)


def sent_and_summed(array, axis, dim):
    count = lax.axis_size(axis)
    pieces = lax.all_to_all(cut_along(array, dim, count), axis, 0, 0, tiled=True)
    return jnp.sum(pieces.astype(jnp.float32), axis=0)


def rms_rows(row_block, gain):
    wide = row_block.astype(jnp.float32)
    factor = lax.rsqrt(jnp.mean(wide * wide, axis=-1, keepdims=True) + norm_eps)
    return (wide * factor * gain).astype(jnp.bfloat16)


def head_norm(outputs, gain):
    factor = lax.rsqrt(jnp.mean(outputs * outputs, axis=-1, keepdims=True) + norm_eps)
    flat = (outputs * factor).reshape(outputs.shape[:-2] + (-1,))
    return (flat * gain).astype(jnp.bfloat16)


def block_terms(q_blk, k_blk, v_blk, g_blk):
    block_len = q_blk.shape[0]
    part_len = min(part_limit, block_len)
    part_count = block_len // part_len
    within = jnp.cumsum(g_blk, axis=0)
    part_ends = within[part_len - 1 :: part_len]
    anchor = jnp.concatenate([jnp.zeros_like(part_ends[:1]), part_ends[:-1]], axis=0)
    q_wide = q_blk.astype(jnp.float32)
    k_wide = k_blk.astype(jnp.float32)
    q_parts = q_wide.reshape((part_count, part_len) + q_blk.shape[1:])
    w_parts = within.reshape((part_count, part_len) + within.shape[1:])
    near_query = (q_parts * jnp.exp(w_parts - anchor[:, None])).astype(jnp.bfloat16)
    near_key = (k_wide[None] * jnp.exp(anchor[:, None] - within[None])).astype(jnp.bfloat16)
    scores = jnp.einsum(
        "itbhk,isbhk->ibhts", near_query, near_key, preferred_element_type=jnp.float32
    )
    row_pos = jnp.arange(part_count)[:, None] * part_len + jnp.arange(part_len)[None]
    keep = row_pos[:, :, None] >= jnp.arange(block_len)[None, None]
    weights = jnp.where(keep[:, None, None], scores, 0.0).astype(jnp.bfloat16)
    in_block = jnp.einsum("ibhts,sbhv->itbhv", weights, v_blk, preferred_element_type=jnp.float32)
    in_block = in_block.reshape((block_len,) + in_block.shape[2:])
    block_total = within[-1]
    start_query = (q_wide * jnp.exp(within)).astype(jnp.bfloat16)
    end_key = (k_wide * jnp.exp(block_total[None] - within)).astype(jnp.bfloat16)
    added = jnp.einsum("sbhk,sbhv->bhkv", end_key, v_blk, preferred_element_type=jnp.float32)
    return (in_block, start_query, block_total, added)


def block_form(query_all, key_all, value_all, decay_all):
    seq_len, batch_size, head_count, width_k = query_all.shape
    width_v = value_all.shape[-1]
    block_count = seq_len // BLOCK

    def to_blocks(tensor):
        return tensor.reshape((block_count, BLOCK) + tensor.shape[1:])

    def advance(carried, inputs):
        states, offset = carried
        in_block, start_query, block_total, added = block_terms(*inputs)
        new_states = jnp.exp(block_total)[..., None] * states + added
        return ((new_states, offset + block_total), (in_block, start_query, states, offset))

    start_states = jnp.zeros((batch_size, head_count, width_k, width_v), jnp.float32)
    start_log = jnp.zeros((batch_size, head_count, width_k), jnp.float32)
    (local_states, totals), (outputs, start_queries, block_starts, block_offsets) = lax.scan(
        advance,
        (start_states, start_log),
        (to_blocks(query_all), to_blocks(key_all), to_blocks(value_all), to_blocks(decay_all)),
    )
    return (outputs, start_queries, block_starts, block_offsets, local_states, totals)


def single_token(query, key_new, value_new, decay, states):
    query = query.astype(jnp.float32)
    key_new = key_new.astype(jnp.float32)
    value_new = value_new.astype(jnp.float32)
    from_state = jnp.einsum("bhk,bhkv->bhv", query * jnp.exp(decay), states)
    token_score = jnp.sum(query * key_new, axis=-1, keepdims=True)
    outputs = from_state + token_score * value_new
    carried = jnp.exp(decay)[..., None] * states + key_new[..., None] * value_new[..., None, :]
    return (outputs, carried)


def chain(earlier, later):
    return (earlier[0] + later[0], jnp.exp(later[0])[..., None] * earlier[1] + later[1])


def on_device(
    pieces,
    new_tokens,
    w_query,
    w_key,
    w_value,
    w_decay,
    decay_bias,
    norm_gain,
    head_gain,
    w_out,
    prompt_state,
    decode_state,
):
    tp_size = lax.axis_size("tp")
    kv_size = lax.axis_size(KV)
    tp_index = lax.axis_index("tp")
    kv_index = lax.axis_index(KV)
    heads_here = w_query.shape[1] // DK
    bias_here = lax.dynamic_slice_in_dim(decay_bias, tp_index * (heads_here * DK), heads_here * DK)
    gain_here = lax.dynamic_slice_in_dim(head_gain, tp_index * (heads_here * DV), heads_here * DV)
    own_pos, prompt_count, width = pieces.shape
    piece_count = own_pos * prompt_count
    normed_piece = rms_rows(pieces, norm_gain).reshape(piece_count, width)
    normed_dec = rms_rows(new_tokens, norm_gain)
    rows_all = jnp.concatenate([normed_piece, normed_dec], axis=0)
    row_count = rows_all.shape[0]
    row_block = collect(rows_all, "tp", 0)
    products = jnp.concatenate(
        [
            jnp.dot(row_block, w_query, preferred_element_type=jnp.float32),
            jnp.dot(row_block, w_key, preferred_element_type=jnp.float32),
            jnp.dot(row_block, w_value, preferred_element_type=jnp.float32),
            jnp.dot(row_block, w_decay, preferred_element_type=jnp.float32),
        ],
        axis=-1,
    )
    products = products.reshape(tp_size, row_count, products.shape[-1])
    piece_prod = products[:, :piece_count].reshape(
        tp_size * own_pos, prompt_count, products.shape[-1]
    )
    dec_prod = products[:, piece_count:].reshape(
        tp_size * (row_count - piece_count), products.shape[-1]
    )

    def split_roles(product):
        lead = product.shape[:-1]
        qk_cols = heads_here * DK
        v_cols = heads_here * DV
        queries = (product[..., :qk_cols] * DK ** (-0.5)).astype(jnp.bfloat16)
        keys_new = product[..., qk_cols : 2 * qk_cols].astype(jnp.bfloat16)
        values_new = product[..., 2 * qk_cols : 2 * qk_cols + v_cols].astype(jnp.bfloat16)
        decays = jax.nn.log_sigmoid(product[..., 2 * qk_cols + v_cols :] + bias_here) / decay_tau
        return (
            queries.reshape(lead + (heads_here, DK)),
            keys_new.reshape(lead + (heads_here, DK)),
            values_new.reshape(lead + (heads_here, DV)),
            decays.reshape(lead + (heads_here, DK)),
        )

    query_p, key_p, value_p, decay_p = split_roles(piece_prod)
    in_blocks, start_queries, block_starts, block_offsets, local_states, totals = block_form(
        query_p, key_p, value_p, decay_p
    )
    whole_start = collect(prompt_state.astype(jnp.bfloat16), KV, 2).astype(prompt_state.dtype)
    prefix_log, prefix_states = entering(
        (totals, local_states), KV, chain, (jnp.zeros_like(totals), jnp.zeros_like(local_states))
    )
    incoming = jnp.exp(prefix_log)[..., None] * whole_start + prefix_states
    full_starts = block_starts + jnp.exp(block_offsets)[..., None] * incoming[None]
    from_state = jnp.einsum("ntbhk,nbhkv->ntbhv", start_queries.astype(jnp.float32), full_starts)
    piece_att = (in_blocks + from_state).reshape((tp_size * own_pos,) + in_blocks.shape[2:])
    rows_k = prompt_state.shape[2]
    block_logs = collect(totals[None], KV, 0)
    later_mask = (jnp.arange(kv_size) > kv_index).astype(jnp.float32)
    suffix_log = jnp.einsum("n,nbhk->bhk", later_mask, block_logs)
    grand_total = jnp.sum(block_logs, axis=0)
    grand_slice = lax.dynamic_slice_in_dim(grand_total, kv_index * rows_k, rows_k, 2)
    summed = sent_and_summed(
        (jnp.exp(suffix_log)[..., None] * local_states).astype(jnp.bfloat16), KV, 2
    )
    prompt_out = summed + jnp.exp(grand_slice)[..., None] * prompt_state
    query_d, key_d, value_d, decay_d = split_roles(dec_prod)
    decode_att, decode_out = single_token(query_d, key_d, value_d, decay_d, decode_state)
    piece_normed = head_norm(piece_att, gain_here)
    dec_normed = head_norm(decode_att, gain_here)
    send_rows = jnp.concatenate(
        [
            piece_normed.reshape(tp_size, piece_count, piece_normed.shape[-1]),
            dec_normed.reshape(tp_size, dec_normed.shape[0] // tp_size, dec_normed.shape[-1]),
        ],
        axis=1,
    )
    mixed = jnp.dot(
        lax.all_to_all(send_rows, "tp", split_axis=0, concat_axis=2, tiled=True),
        w_out,
        preferred_element_type=jnp.float32,
    ).astype(jnp.bfloat16)
    mixed_piece = mixed[0, :piece_count].reshape(own_pos, prompt_count, mixed.shape[-1])
    mixed_decode = mixed[0, piece_count:]
    return (mixed_piece, mixed_decode, prompt_out, decode_out)


def solution(mesh):
    finer = Mesh(
        mesh.devices.reshape(mesh.shape["dp"], 4, 4, mesh.shape["tp"]), ("dp", "kv_0", "kv_1", "tp")
    )
    return jax.shard_map(
        on_device,
        mesh=finer,
        in_specs=(
            P(KV_TP, "dp", None),
            P(DP_KV_TP, None),
            P(None, "tp"),
            P(None, "tp"),
            P(None, "tp"),
            P(None, "tp"),
            P(),
            P(),
            P(),
            P(),
            P("dp", "tp", KV, None),
            P(DP_KV, "tp", None, None),
        ),
        out_specs=(
            P(KV_TP, "dp", None),
            P(DP_KV_TP, None),
            P("dp", "tp", KV, None),
            P(DP_KV, "tp", None, None),
        ),
        check_vma=False,
    )
```

profile of v0, /device:TPU:1, one launch (start us, length us, event | category | flops | bytes accessed | tf_op | source)
XLA Modules:
  0.0 267.0 jit_solution(8254493999903162582)
XLA Ops:
  8.2 2.4 fusion.33
  11.4 3.4 %fusion.35 = bf16[128,2,2048]{2,1,0:T(2,128)(2,1)} fusion(bf16[128,2,2048]{2,1,0:T(2,128)(2,1)} %param.14, f32[2048]{0:T(1024)} %param.21, f32[128,2]{1,0:T(8,128)S(1)} %add_rsqrt_fusion), kind=kLoop, calls=%fused_computation.55 | loop fusion | flops 2097152 | bytes 2106368 | tf_op jit(solution)/shard_map/convert_element_type | solution.py:73
  14.8 1.5 reshape.346
  16.4 1.6 broadcast_in_dim.54
  17.9 6.2 %all-to-all-start = ((bf16[2,258,2048]{2,1,0:T(8,128)(2,1)}), bf16[2,258,2048]{2,1,0:T(8,128)(2,1)}, u32[]{:S(2)}, u32[]{:S(2)}) async-start(bf16[2,258,2048]{2,1,0:T(8,128)(2,1)} %broadcast_in_dim.54), calls=%async_computation | async-start | bytes 4325376 | tf_op jit(solution)/shard_map/all_to_all | solution.py:23
  24.2 2.7 all-to-all-done
  26.8 3.3 %reshape.347 = bf16[516,2048]{1,0:T(8,128)(2,1)} reshape(bf16[2,258,2048]{2,1,0:T(8,128)(2,1)} %all-to-all-done) | data formatting | bytes 4227072 | tf_op jit(solution)/shard_map/reshape | solution.py:29
  30.2 3.0 %fusion.73 = f32[516,512]{1,0:T(8,128)S(1)} fusion(bf16[516,2048]{1,0:T(8,128)(2,1)} %reshape.347, bf16[2048,512]{1,0:T(8,128)(2,1)S(1)} %copy-done), kind=kOutput, calls=%fused_computation.144 | convolution fusion | flops 1082130432 | bytes 5267456 | tf_op jit(solution)/shard_map/dot_general | solution.py:182
  33.7 2.4 fusion.72
  36.1 1.3 fusion.71
  37.7 1.3 fusion.70
  38.9 2.8 %pad_maximum_fusion = f32[516,2560]{1,0:T(8,128)} fusion(f32[516,512]{1,0:T(8,128)S(1)} %fusion.73, f32[516,1024]{1,0:T(8,128)S(1)} %fusion.72, f32[516,512]{1,0:T(8,128)S(1)} %fusion.71, f32[516,512]{1,0:T(8,128)S(1)} %fusion.70), kind=kLoop, calls=%fused_computation.43 | loop fusion | flops 3962880 | bytes 10567680 | tf_op jit(solution)/shard_map/concatenate | solution.py:177
  41.7 5.4 %reshape.348 = f32[2,258,2560]{2,1,0:T(8,128)} reshape(f32[516,2560]{1,0:T(8,128)} %pad_maximum_fusion) | data formatting | bytes 10567680 | tf_op jit(solution)/shard_map/reshape | solution.py:186
  47.1 5.1 %slice.138 = f32[2,256,2560]{2,1,0:T(8,128)} slice(f32[2,258,2560]{2,1,0:T(8,128)} %reshape.348), slice={[0:2], [0:256], [0:2560]} | slice | bytes 10485760 | tf_op jit(solution)/shard_map/slice | solution.py:187
  52.2 7.4 %reshape.349 = f32[256,2,2560]{2,1,0:T(2,128)} reshape(f32[2,256,2560]{2,1,0:T(8,128)} %slice.138) | data formatting | bytes 10485760 | tf_op jit(solution)/shard_map/reshape | solution.py:187
  59.7 2.4 slice.140
  62.0 2.3 slice.141
  64.5 4.8 %fusion.51 = (bf16[256,2,512]{2,1,0:T(2,128)(2,1)}, f32[256,2,512]{2,1,0:T(2,128)S(1)}) fusion(f32[256,2,2560]{2,1,0:T(2,128)} %reshape.349, f32[512]{0:T(512)S(1)} %dynamic_slice.24), kind=kLoop, calls=%fused_computation.85 | loop fusion | flops 3145728 | bytes 3672064 | tf_op jit(solution)/shard_map/convert_element_type | solution.py:198
  69.2 2.0 reshape_reshape.12
  73.5 1.6 reshape_reshape.14
  75.1 1.1 reshape_reshape.15
  76.3 36.5 %while.21 = (s32[]{:T(128)}, f32[2,4,128,256]{3,2,1,0:T(8,128)S(1)}, f32[2,4,128]{2,1,0:T(4,128)S(1)}, f32[4,64,2,4,256]{4,1,3,2,0:T(8,128)}, bf16[4,64,2,4,128]...) while((s32[]{:T(128)}, ...), condition=%wide.region_4.5_spmd.clone, body=%wide.region_2.4_spmd.clone.sunk | while | flops 65543236 | bytes 11581150 | solution.py:126
  76.3 1.1 bitcast_dynamic-update-slice_fusion.4
  77.4 1.1 fusion.99
  86.5 1.1 fusion.99
  103.6 1.1 bitcast_dynamic-update-slice_fusion.4
  113.8 9.8 %all-gather = f32[8,4,128]{2,1,0:T(4,128)S(1)} all-gather(f32[2,4,128]{2,1,0:T(4,128)S(1)} %get-tuple-element.69), channel_id=2, replica_groups=mesh['dp'=4,'kv_0'=4,'kv_1'=4,'tp'=2] {'kv_1'}, dimensions={0}, use_global_device_ids=true | all-gather | bytes 20480 | tf_op jit(solution)/shard_map/all_gather | solution.py:48
  123.6 40.6 %all-gather.7.cloned.1.call-done = f32[8,4,128,256]{3,2,1,0:T(8,128)} async-done(((f32[2,4,128,256]{3,2,1,0:T(8,128)}), f32[8,4,128,256]{3,2,1,0:T(8,128)}) %all-gather.7.cloned.1.call-update) | async-done | bytes 4194320 | tf_op jit(solution)/shard_map/all_gather | solution.py:48
  164.2 3.3 %fusion.47 = f32[1,2,4,128,256]{4,3,2,1,0:T(8,128)} fusion(f32[8,4,128,256]{3,2,1,0:T(8,128)} %all-gather.7.cloned.1.call-done, f32[2,4,128]{2,1,0:T(4,128)S(1)} %get-tuple-element.226, f32[2,4,128]{2,1,0:T(4,128)S(1)} %get-tuple-element.223, f32[2,4,128]{2,1,0:T(4,128)S(1)} %get-tuple-element.225, f32[2,4,128]{2,1,0:T(4,128)S(1)} %get-tuple-element.224), kind=kLoop, calls=%fused_computation.77 | loop fusion | flops 1835008 | bytes 5259264 | tf_op jit(solution)/shard_map/add | solution.py:146
  168.1 5.8 %all-to-all-start.3 = ((f32[16,1,2,4,128]{4,3,2,1,0:T(4,128)}), f32[16,1,2,4,128]{4,3,2,1,0:T(4,128)S(1)}, u32[]{:S(2)}, u32[]{:S(2)}) async-start(f32[16,1,2,4,128]{4,3,2,1,0:T(4,128)} %broadcast_in_dim.56), calls=%async_computation.3 | async-start | bytes 131072 | tf_op jit(solution)/shard_map/all_to_all | solution.py:23
  175.1 1.8 fusion.74
  177.3 10.7 %all_gather.22 = f32[4,2,4,128]{3,2,1,0:T(4,128)S(1)} all-gather(f32[1,2,4,128]{3,2,1,0:T(4,128)S(1)} %get-tuple-element.222), channel_id=1, replica_groups=mesh['dp'=4,'kv_0'=4,'kv_1'=4,'tp'=2] {'kv_0'}, dimensions={0}, use_global_device_ids=true | all-gather | bytes 20480 | tf_op jit(solution)/shard_map/all_gather | solution.py:48
  189.2 6.1 %all-to-all-start.4 = ((bf16[16,2,4,8,256]{4,3,2,1,0:T(8,128)(2,1)}), bf16[16,2,4,8,256]{4,3,2,1,0:T(8,128)(2,1)S(1)}, u32[]{:S(2)}, u32[]{:S(2)}) async-start(bf16[16,2,4,8,256]{4,3,2,1,0:T(8,128)(2,1)} %copy.127), calls=%async_computation.4 | async-start | bytes 1048576 | tf_op jit(solution)/shard_map/all_to_all | solution.py:66
  195.4 8.8 %all-to-all-done.4 = bf16[16,2,4,8,256]{4,3,2,1,0:T(8,128)(2,1)S(1)} async-done(((bf16[16,2,4,8,256]{4,3,2,1,0:T(8,128)(2,1)}), bf16[16,2,4,8,256]{4,3,2,1,0:T(8,128)(2,1)S(1)}, u32[]{:S(2)}, u32[]{:S(2)}) %all-to-all-start.4) | async-done | bytes 524320 | tf_op jit(solution)/shard_map/all_to_all | solution.py:66
  205.9 4.5 %all-to-all-start.1 = ((bf16[16,2,4,8,256]{4,3,2,1,0:T(8,128)(2,1)}), bf16[16,2,4,8,256]{4,3,2,1,0:T(8,128)(2,1)S(1)}, u32[]{:S(2)}, u32[]{:S(2)}) async-start(bf16[16,2,4,8,256]{4,3,2,1,0:T(8,128)(2,1)} %broadcast_in_dim.55), calls=%async_computation.1 | async-start | bytes 1048576 | tf_op jit(solution)/shard_map/all_to_all | solution.py:23
  210.5 1.7 multiply_add_fusion
  212.1 7.3 %all-to-all-done.1 = bf16[16,2,4,8,256]{4,3,2,1,0:T(8,128)(2,1)S(1)} async-done(((bf16[16,2,4,8,256]{4,3,2,1,0:T(8,128)(2,1)}), bf16[16,2,4,8,256]{4,3,2,1,0:T(8,128)(2,1)S(1)}, u32[]{:S(2)}, u32[]{:S(2)}) %all-to-all-start.1) | async-done | bytes 524320 | tf_op jit(solution)/shard_map/all_to_all | solution.py:23
  219.4 8.3 %all-gather.5.cloned.1.call-done = f32[4,2,4,128,256]{4,3,2,1,0:T(8,128)} async-done(((f32[1,2,4,128,256]{4,3,2,1,0:T(8,128)}), f32[4,2,4,128,256]{4,3,2,1,0:T(8,128)}) %all-gather.5.cloned.1.call-update) | async-done | bytes 4194320 | tf_op jit(solution)/shard_map/all_gather | solution.py:48
  227.7 5.5 %fusion.46 = f32[2,4,128,256]{3,2,1,0:T(8,128)S(1)} fusion(f32[4,2,4,128,256]{4,3,2,1,0:T(8,128)} %all-gather.5.cloned.1.call-done, f32[8,4,128,256]{3,2,1,0:T(8,128)} %all-gather.7.cloned.1.call-done, bf16[16,2,4,8,256]{4,3,2,1,0:T(8,128)(2,1)S(1)} %all-to-all-done.1, f32[2,4,128]{2,1,0:T(4,128)S(1)} %get-tuple-element.225, ...), kind=kLoop, calls=%fused_computation.72 | loop fusion | flops 7077888 | bytes 10002440 | tf_op jit(solution)/shard_map/mul | solution.py:218
  233.3 1.9 multiply_reduce_fusion
  235.2 2.7 %copy.123 = f32[4,64,2,4,256]{4,3,2,1,0:T(4,128)} copy(f32[4,64,2,4,256]{4,1,3,2,0:T(8,128)S(1)} %get-tuple-element.230) | data formatting | bytes 4194304 | tf_op jit(solution)/shard_map/add | solution.py:220
  237.8 2.3 reshape.350
  240.4 1.9 mul.353
  242.3 3.3 %mul.354 = f32[2,256,1024]{2,1,0:T(8,128)} reshape(f32[256,2,4,256]{3,2,1,0:T(4,128)} %mul.353) | data formatting | bytes 4194304 | tf_op jit(solution)/shard_map/mul | solution.py:78
  245.6 2.3 multiply_convert_fusion.4
  248.0 5.3 %all_to_all.35 = bf16[2,258,1024]{2,1,0:T(8,128)(2,1)S(1)} all-to-all(bf16[2,258,1024]{2,1,0:T(8,128)(2,1)S(1)} %pad_maximum_fusion.2), channel_id=1, replica_groups=mesh['dp'=4,'kv_0'=4,'kv_1'=4,'tp'=2] {'tp'}, dimensions={0} | all-to-all | bytes 2113536 | tf_op jit(solution)/shard_map/all_to_all | solution.py:243
  255.6 2.5 fusion.32
  258.7 1.5 reshape_squeeze.3
  (180 shorter events, 46.1 us)
Async XLA Ops:
  7.2 23.0 %copy-start = (bf16[2048,512]{1,0:T(8,128)(2,1)S(1)}, bf16[2048,512]{1,0:T(8,128)(2,1)}, u32[]{:S(2)}) copy-start(bf16[2048,512]{1,0:T(8,128)(2,1)} %param.19) | copy-start | bytes 6291460
  17.9 8.9 %all-to-all-start = ((bf16[2,258,2048]{2,1,0:T(8,128)(2,1)}), bf16[2,258,2048]{2,1,0:T(8,128)(2,1)}, u32[]{:S(2)}, u32[]{:S(2)}) async-start(bf16[2,258,2048]{2,1,0:T(8,128)(2,1)} %broadcast_in_dim.54), calls=%async_computation | async-start | bytes 4325376 | tf_op jit(solution)/shard_map/all_to_all | solution.py:23
  24.2 140.0 %all-gather.7.cloned.1.call-start = ((), (), s32[]{:S(2)}) async-start(), calls=%async_computation.6 | async-start | bytes 5242880 | tf_op jit(solution)/shard_map/all_gather | solution.py:48
  30.2 3.0 %copy-start.6 = (bf16[516,2048]{1,0:T(8,128)(2,1)S(1)}, bf16[516,2048]{1,0:T(8,128)(2,1)}, u32[]{:S(2)}) copy-start(bf16[516,2048]{1,0:T(8,128)(2,1)} %reshape.347) | copy-start | bytes 6340612
  30.2 3.5 %copy-start.13 = (bf16[2048,1024]{1,0:T(8,128)(2,1)S(1)}, bf16[2048,1024]{1,0:T(8,128)(2,1)}, u32[]{:S(2)}) copy-start(bf16[2048,1024]{1,0:T(8,128)(2,1)} %param.18) | copy-start | bytes 12582916
  33.6 2.4 copy-start.14
  36.1 1.6 copy-start.15
  59.7 4.7 %copy-start.12 = (f32[1024]{0:T(1024)S(1)}, f32[1024]{0:T(1024)}, u32[]{:S(2)}) copy-start(f32[1024]{0:T(1024)} %param.20) | copy-start | bytes 12292
  73.5 1.6 copy-start.8
  112.8 1.0 copy-start.2
  113.8 114.0 %all-gather.5.cloned.1.call-start = ((), (), s32[]{:S(2)}) async-start(), calls=%async_computation.5 | async-start | bytes 5242880 | tf_op jit(solution)/shard_map/all_gather | solution.py:48
  167.5 9.8 %copy-start.11 = (f32[2048]{0:T(1024)S(1)}, f32[2048]{0:T(1024)}, u32[]{:S(2)}) copy-start(f32[2048]{0:T(1024)} %param.22) | copy-start | bytes 24580
  167.5 20.6 %copy-start.3 = (f32[2,4,128,256]{3,2,1,0:T(8,128)S(1)}, f32[2,4,128,256]{3,2,1,0:T(8,128)}, u32[]{:S(2)}) copy-start(f32[2,4,128,256]{3,2,1,0:T(8,128)} %copy-done.2) | copy-start | bytes 3145732
  168.1 19.8 %all-to-all-start.3 = ((f32[16,1,2,4,128]{4,3,2,1,0:T(4,128)}), f32[16,1,2,4,128]{4,3,2,1,0:T(4,128)S(1)}, u32[]{:S(2)}, u32[]{:S(2)}) async-start(f32[16,1,2,4,128]{4,3,2,1,0:T(4,128)} %broadcast_in_dim.56), calls=%async_computation.3 | async-start | bytes 131072 | tf_op jit(solution)/shard_map/all_to_all | solution.py:23
  188.1 16.3 %copy-start.10 = (f32[2,4,8,256]{3,2,1,0:T(8,128)S(1)}, f32[2,4,8,256]{3,2,1,0:T(8,128)}, u32[]{:S(2)}) copy-start(f32[2,4,8,256]{3,2,1,0:T(8,128)} %param.24) | copy-start | bytes 196612
  188.3 22.1 %copy-start.4 = (f32[4,4,128,256]{3,2,1,0:T(8,128)S(1)}, f32[4,4,128,256]{3,2,1,0:T(8,128)}, u32[]{:S(2)}) copy-start(f32[4,4,128,256]{3,2,1,0:T(8,128)} %param.25) | copy-start | bytes 6291460
  189.2 15.1 %all-to-all-start.4 = ((bf16[16,2,4,8,256]{4,3,2,1,0:T(8,128)(2,1)}), bf16[16,2,4,8,256]{4,3,2,1,0:T(8,128)(2,1)S(1)}, u32[]{:S(2)}, u32[]{:S(2)}) async-start(bf16[16,2,4,8,256]{4,3,2,1,0:T(8,128)(2,1)} %copy.127), calls=%async_computation.4 | async-start | bytes 1048576 | tf_op jit(solution)/shard_map/all_to_all | solution.py:66
  205.9 13.5 %all-to-all-start.1 = ((bf16[16,2,4,8,256]{4,3,2,1,0:T(8,128)(2,1)}), bf16[16,2,4,8,256]{4,3,2,1,0:T(8,128)(2,1)S(1)}, u32[]{:S(2)}, u32[]{:S(2)}) async-start(bf16[16,2,4,8,256]{4,3,2,1,0:T(8,128)(2,1)} %broadcast_in_dim.55), calls=%async_computation.1 | async-start | bytes 1048576 | tf_op jit(solution)/shard_map/all_to_all | solution.py:23
  227.7 5.5 %copy-start.5 = (f32[4,2,4,128,256]{4,3,2,1,0:T(8,128)S(1)}, f32[4,2,4,128,256]{4,3,2,1,0:T(8,128)}, u32[]{:S(2)}) copy-start(f32[4,2,4,128,256]{4,3,2,1,0:T(8,128)} %get-tuple-element.67) | copy-start | bytes 12582916
  227.7 5.5 %copy-start.7 = (f32[4,64,2,4,256]{4,1,3,2,0:T(8,128)S(1)}, f32[4,64,2,4,256]{4,1,3,2,0:T(8,128)}, u32[]{:S(2)}) copy-start(f32[4,64,2,4,256]{4,1,3,2,0:T(8,128)} %get-tuple-element.66) | copy-start | bytes 6291460
  227.7 5.5 %copy-start.9 = (bf16[4,64,2,4,128]{4,1,3,2,0:T(8,128)(2,1)S(1)}, bf16[4,64,2,4,128]{4,1,3,2,0:T(8,128)(2,1)}, u32[]{:S(2)}) copy-start(bf16[4,64,2,4,128]{4,1,3,2,0:T(8,128)(2,1)} %get-tuple-element.71) | copy-start | bytes 1572868
  245.6 9.9 %slice-start = ((s8[8388608]{0:T(1024)(128)(4,1)}), s8[4194304]{0:T(1024)(128)(4,1)S(1)}, s32[]{:S(2)}) async-start(s8[8388608]{0:T(1024)(128)(4,1)} %bitcast.198), calls=%async_computation.7 | async-start | bytes 8388608
  248.0 7.5 %slice-start.1 = ((s8[8388608]{0:T(1024)(128)(4,1)}), s8[4194304]{0:T(1024)(128)(4,1)S(1)}, s32[]{:S(2)}) async-start(s8[8388608]{0:T(1024)(128)(4,1)} %bitcast.198), calls=%async_computation.8 | async-start | bytes 8388608
  255.5 4.7 %copy-start.1 = (bf16[2048,512]{1,0:T(8,128)(2,1)S(1)}, bf16[2048,512]{1,0:T(8,128)(2,1)}, u32[]{:S(2)}) copy-start(bf16[2048,512]{1,0:T(8,128)(2,1)} %param.19) | copy-start | bytes 6291460
Sparse Core Ops, SparseCore 0:
  113.9 50.2 all-gather.6
  167.6 60.0 all-gather.4
where the time goes:
time: 269 us; the launch traced here: 267 us
  waiting for transfers between devices  67.7 us (25%)
  local copies, waits for them, and re-layouts  67 us (25%)
  other arithmetic  50.6 us (19%)
  blocking collectives  25.7 us (10%)
  starting transfers between devices  22.6 us (8%)
  matrix products  18.5 us (7%)
  between operations  14.5 us (5%)
    all_gather x2, waiting for transfers between devices, entering(): pieces = jax.tree.map(lambda part: lax.all_gather(part, axis), subtotal)  48.9 us
    all_gather x2, blocking collectives, entering(): pieces = jax.tree.map(lambda part: lax.all_gather(part, axis), subtotal)  20.4 us
    all_to_all x3, starting transfers between devices, copy_for_each(): return lax.all_to_all(copies, axis, split_axis=0, concat_axis=0, tiled=True)  16.5 us
    all_to_all x3, waiting for transfers between devices, copy_for_each(): return lax.all_to_all(copies, axis, split_axis=0, concat_axis=0, tiled=True)  9.95 us
    all_to_all x1, waiting for transfers between devices, sent_and_summed(): lax.all_to_all(cut_along(array, dim, count), axis, 0, 0, tiled=True)  8.83 us
    reshape x1, local copies, waits for them, and re-layouts, on_device(): products[:, :piece_count]  7.42 us
    dynamic_update_slice x8, local copies, waits for them, and re-layouts, block_form(): lax.scan(advance, (start_states, start_log), (to_blocks(query_all), to_bl...  6.08 us
    all_to_all x1, starting transfers between devices, sent_and_summed(): lax.all_to_all(cut_along(array, dim, count), axis, 0, 0, tiled=True)  6.08 us
  transfers between devices with their start and end apart: 6, of which 5 were waited for; matrix products, arithmetic and copies ran while one was open for 3% of the time, Pallas kernels for 0%

commit v1 on v0

v1 whole, which is shorter than its diff:
```python
import functools

import jax
import jax.numpy as jnp
from jax import lax
from jax.experimental import pallas as pl
from jax.experimental.pallas import tpu as pltpu
from jax.sharding import PartitionSpec as P

F32 = jnp.float32
BF16 = jnp.bfloat16
MESH = pl.DeviceIdType.MESH

DK = 128
DV = 256
EPS = 0.1
TAU = 16.0
SUB = 16
BLK = 64
HEADS = 4
PR = 2
OWN = 128
PAD = 16
RP = PR * OWN
ROWS = RP + PAD
KVN = 16
PH = PR * HEADS
TN = (((0,), (0,)), ((), ()))
NT = (((1,), (1,)), ((), ()))


def dot(a, b):
    return jnp.dot(a, b, preferred_element_type=F32)


def dotg(a, b, dims):
    return lax.dot_general(a, b, dims, preferred_element_type=F32)


def log_decay(x):
    return (jnp.minimum(x, 0.0) - jnp.log1p(jnp.exp(-jnp.abs(x)))) / TAU


def order_matrix():
    m = lax.broadcasted_iota(jnp.int32, (RP, RP), 0)
    n = lax.broadcasted_iota(jnp.int32, (RP, RP), 1)
    first = jnp.where(m < OWN, PR * m, PR * (m - OWN) + 1)
    return jnp.where(n == first, 1.0, 0.0).astype(BF16)


def attend_kernel(
    pieces, new_tokens, w_query, w_key, w_value, w_decay, bias, gain, head_gain, prompt_state, decode_state,
    own_out, peer_out, prompt_out, dec_key, dec_value, dec_decay,
    x3, nt, wq, wk, wv, wd, bias_v, gain_v, hg_v, ps, ds, xs, rows, qb, kb, vb, db, bb, st, tt, ttt, rs, rt, sb, inc, att,
    sqc, nrm, load_sem, row_sem, st_send, st_recv, tt_send, tt_recv, in_send, in_recv, nrm_sem,
):
    kv = lax.axis_index("kv")
    tp = lax.axis_index("tp")
    other = 1 - tp

    loads = [
        pltpu.make_async_copy(src, dst, load_sem.at[i])
        for i, (src, dst) in enumerate(
            [
                (pieces, x3), (new_tokens, nt), (gain, gain_v), (w_decay, wd), (w_key, wk), (w_value, wv),
                (bias, bias_v), (w_query, wq), (prompt_state, ps), (decode_state, ds), (head_gain, hg_v),
            ]
        )
    ]
    for copy in loads:
        copy.start()

    barrier = pltpu.get_barrier_semaphore()
    pl.semaphore_signal(barrier, inc=1, device_id={"tp": other}, device_id_type=MESH)
    for d in range(1, KVN):
        pl.semaphore_signal(barrier, inc=1, device_id={"kv": lax.rem(kv + d, KVN)}, device_id_type=MESH)

    order = order_matrix()
    for copy in loads[:3]:
        copy.wait()
    flat = x3[...].reshape(RP, x3.shape[-1])
    width = flat.shape[-1]
    step = 512
    squares = jnp.zeros((RP, 1), F32)
    for c in range(width // step):
        part = dot(order, flat[:, c * step : (c + 1) * step])
        xs[:, c * step : (c + 1) * step] = part
        squares += jnp.sum(part * part, axis=-1, keepdims=True)
    factor = lax.rsqrt(squares / width + EPS)
    for c in range(width // step):
        cols = slice(c * step, (c + 1) * step)
        rows[tp, :RP, cols] = (xs[:, cols] * factor * gain_v[:, cols]).astype(BF16)
    wide = nt[...].astype(F32)
    nt_factor = lax.rsqrt(jnp.sum(wide * wide, axis=-1, keepdims=True) / width + EPS)
    nt_rows = wide * nt_factor * gain_v[...]
    rows[tp, RP:, :] = jnp.concatenate([nt_rows, jnp.zeros((PAD - nt_rows.shape[0], width), F32)], axis=0).astype(BF16)

    pl.semaphore_wait(barrier, KVN)
    row_copy = pltpu.make_async_remote_copy(
        src_ref=rows.at[tp], dst_ref=rows.at[tp], send_sem=row_sem.at[0], recv_sem=row_sem.at[1],
        device_id={"tp": other}, device_id_type=MESH,
    )
    row_copy.start()

    def project(half, weights, out, kind):
        per = 2 * DK

        def tile(j, _):
            cols = pl.ds(pl.multiple_of(j * per, per), per)
            got = dot(rows[half], weights[:, cols])
            if kind == "v":
                out[j, half] = got.astype(BF16)
            else:
                for e in range(2):
                    part = got[:, e * DK : (e + 1) * DK]
                    if kind == "q":
                        part = (part * DK**-0.5).astype(BF16)
                    elif kind == "k":
                        part = part.astype(BF16)
                    else:
                        at = pl.multiple_of(tp * (HEADS * DK) + j * per + e * DK, DK)
                        part = log_decay(part + bias_v[:, pl.ds(at, DK)])
                    out[2 * j + e, half] = part
            return 0

        lax.fori_loop(0, weights.shape[1] // per, tile, 0)

    for i in (3, 4, 5, 6):
        loads[i].wait()
    project(tp, wd, db, "d")
    project(tp, wk, kb, "k")
    project(tp, wv, vb, "v")
    row_copy.wait()
    project(other, wd, db, "d")
    project(other, wk, kb, "k")
    project(other, wv, vb, "v")

    t_at = lax.broadcasted_iota(jnp.int32, (OWN, OWN), 0)
    s_at = lax.broadcasted_iota(jnp.int32, (OWN, OWN), 1)
    lower = jnp.where(t_at >= s_at, 1.0, 0.0).astype(BF16)
    lower2 = jnp.concatenate([lower, lower], axis=1)

    def sums(i, _):
        half, p = i // PR, i % PR
        at = pl.ds(pl.multiple_of(p * OWN, OWN), OWN)
        g = jnp.concatenate([db[h, half, at] for h in range(HEADS)], axis=1)
        hi = g.astype(BF16)
        lo = (g - hi.astype(F32)).astype(BF16)
        got = dot(lower2, jnp.concatenate([hi, lo], axis=0))
        for h in range(HEADS):
            bb[h, half, p] = got[:, h * DK : (h + 1) * DK]
        return 0

    lax.fori_loop(0, 2 * PR, sums, 0)

    tt[...] = jnp.zeros_like(tt)

    def add_state(p, _):
        at = pl.ds(pl.multiple_of(p * OWN, OWN), OWN)
        for h in range(HEADS):
            b0, b1 = bb[h, 0, p], bb[h, 1, p]
            t0, t1 = b0[OWN - 1 :], b1[OWN - 1 :]
            e0 = kb[h, 0, at].astype(F32) * jnp.exp((t0 - b0) + t1)
            e1 = kb[h, 1, at].astype(F32) * jnp.exp(t1 - b1)
            keys = jnp.concatenate([e0.astype(BF16), e1.astype(BF16)], axis=0)
            vals = jnp.concatenate([vb[h, 0, at], vb[h, 1, at]], axis=0)
            state = dotg(keys, vals, TN)
            st[:, p * HEADS + h] = state.reshape(KVN, DK // KVN, DV).astype(BF16)
            tt[pl.ds(p * HEADS + h, 1), :] = t0 + t1
        return 0

    lax.fori_loop(0, PR, add_state, 0)
    ttt[...] = tt[...].T.reshape(KVN, DK // KVN, DK)

    def state_copy(to, slot):
        return pltpu.make_async_remote_copy(
            src_ref=st.at[to], dst_ref=rs.at[slot], send_sem=st_send.at[to], recv_sem=st_recv.at[slot],
            device_id={"kv": to}, device_id_type=MESH,
        )

    def total_copy(to, slot):
        return pltpu.make_async_remote_copy(
            src_ref=ttt.at[to], dst_ref=rt.at[slot], send_sem=tt_send.at[to], recv_sem=tt_recv.at[slot],
            device_id={"kv": to}, device_id_type=MESH,
        )

    def back_copy(to, slot):
        return pltpu.make_async_remote_copy(
            src_ref=sb.at[to], dst_ref=inc.at[slot], send_sem=in_send.at[to], recv_sem=in_recv.at[slot],
            device_id={"kv": to}, device_id_type=MESH,
        )

    for d in range(1, KVN):
        to = lax.rem(kv + d, KVN)
        total_copy(to, kv).start()
        state_copy(to, kv).start()
    rs[kv] = st[kv]
    rt[kv] = ttt[kv]

    loads[7].wait()
    project(0, wq, qb, "q")
    project(1, wq, qb, "q")

    t_in = lax.broadcasted_iota(jnp.int32, (BLK, BLK), 0)
    s_in = lax.broadcasted_iota(jnp.int32, (BLK, BLK), 1)
    keep = t_in >= s_in

    def inside(i, _):
        p, h = i // HEADS, i % HEADS
        at = pl.ds(pl.multiple_of(p * OWN, OWN), OWN)
        ks = [kb[h, half, at].astype(F32) for half in range(2)]
        qs = [qb[h, half, at].astype(F32) for half in range(2)]
        bs = [bb[h, half, p] for half in range(2)]
        vs = [vb[h, half, at] for half in range(2)]
        m0, t0 = bs[0][BLK - 1 : BLK], bs[0][OWN - 1 :]
        m1 = bs[1][BLK - 1 : BLK]
        first = (ks[0][:BLK] * jnp.exp(m0 - bs[0][:BLK])).astype(BF16)
        state1 = dotg(first, vs[0][:BLK], TN)
        second = ks[0] * jnp.exp(t0 - bs[0])
        state2 = dotg(second.astype(BF16), vs[0], TN)
        third = jnp.concatenate(
            [(ks[0] * jnp.exp((t0 - bs[0]) + m1)).astype(BF16), (ks[1][:BLK] * jnp.exp(m1 - bs[1][:BLK])).astype(BF16)], axis=0
        )
        state3 = dotg(third, jnp.concatenate([vs[0], vs[1][:BLK]], axis=0), TN)
        starts = [None, state1, state2, state3]
        for blk in range(4):
            half, lo = blk // 2, (blk % 2) * BLK
            b = bs[half][lo : lo + BLK]
            q = qs[half][lo : lo + BLK]
            k = ks[half][lo : lo + BLK]
            v = vs[half][lo : lo + BLK]
            ref = [jnp.zeros((1, DK), F32) if lo == 0 else bs[half][lo - 1 : lo]]
            for n in range(1, BLK // SUB):
                ref.append(b[n * SUB - 1 : n * SUB])
            zero = jnp.zeros((SUB, DK), BF16)
            q_rows, k_cols = [], []
            for n in range(BLK // SUB):
                end = (n + 1) * SUB
                near_q = (q[n * SUB : end] * jnp.exp(b[n * SUB : end] - ref[n])).astype(BF16)
                near_k = (k[:end] * jnp.exp(ref[n] - b[:end])).astype(BF16)
                q_rows.append(jnp.concatenate([near_q if m == n else zero for m in range(BLK // SUB)], axis=1))
                k_cols.append(jnp.concatenate([near_k] + [zero] * (BLK // SUB - 1 - n), axis=0))
            scores = dotg(jnp.concatenate(q_rows, axis=0), jnp.concatenate(k_cols, axis=1), NT)
            weights = jnp.where(keep, scores, 0.0).astype(BF16)
            if blk == 0:
                out = dot(weights, v)
            else:
                start_q = (q * jnp.exp(b - ref[0])).astype(BF16)
                out = dot(
                    jnp.concatenate([start_q, weights], axis=1),
                    jnp.concatenate([starts[blk].astype(BF16), v], axis=0),
                )
            att[i, half, lo : lo + BLK] = out
        sqc[i, 0] = (qs[0] * jnp.exp(bs[0])).astype(BF16)
        sqc[i, 1] = (qs[1] * jnp.exp(bs[1] + t0)).astype(BF16)
        return 0

    lax.fori_loop(0, PH, inside, 0)

    for i in (8, 9, 10):
        loads[i].wait()

    def normed(out, h):
        scale = lax.rsqrt(jnp.sum(out * out, axis=-1, keepdims=True) / DV + EPS)
        gain_at = pl.multiple_of(tp * (HEADS * DV) + h * DV, DV)
        return (out * scale * hg_v[:, pl.ds(gain_at, DV)]).astype(BF16)

    tt[...] = jnp.zeros_like(tt)
    each = 2
    for half in range(2):
        for h in range(HEADS):
            q = qb[h, half, RP:].astype(F32)
            k = kb[h, half, RP:].astype(F32)
            v = vb[h, half, RP:].astype(F32)
            eg = jnp.exp(db[h, half, RP:])
            eq = (q * eg).astype(BF16)
            row = lax.broadcasted_iota(jnp.int32, (PAD, 1), 0)
            out = jnp.sum(q * k, axis=-1, keepdims=True) * v
            for r in range(each):
                from_state = dot(eq, ds[each * half + r, h].astype(BF16))
                out = out + jnp.where(row == r, from_state, 0.0)
                tt[pl.ds((each * half + r) * HEADS + h, 1), :] = eg[r : r + 1]
            nrm[half, RP:, h * DV : (h + 1) * DV] = normed(out, h)
            dec_key[half, h] = kb[h, half, RP:]
            dec_value[half, h] = vb[h, half, RP:]
    dec_decay[...] = tt[...].T

    def scan_step(i, state):
        @pl.when(i != kv)
        def _():
            total_copy(i, i).wait_recv()
            state_copy(i, i).wait_recv()

        sb[i] = state.astype(BF16)

        @pl.when(i != kv)
        def _():
            back_copy(i, kv).start()

        decay = jnp.exp(rt[i])
        return jnp.stack(
            [decay[:, n : n + 1] * state[n] + rs[i, n].astype(F32) for n in range(PH)], axis=0
        )

    prompt_out[...] = lax.fori_loop(0, KVN, scan_step, ps[...])
    inc[kv] = sb[kv]
    for d in range(1, KVN):
        frm = lax.rem(kv + d, KVN)
        back_copy(frm, frm).wait_recv()

    def finish(i, _):
        p, h = i // HEADS, i % HEADS
        incoming = inc[:, i].astype(F32).reshape(DK, DV).astype(BF16)
        at = pl.ds(pl.multiple_of(p * OWN, OWN), OWN)
        cols = pl.ds(pl.multiple_of(h * DV, DV), DV)
        for half in range(2):
            out = att[i, half] + dot(sqc[i, half], incoming)
            nrm[half, at, cols] = normed(out, h)
        return 0

    lax.fori_loop(0, PH, finish, 0)

    nrm_copy = pltpu.make_async_remote_copy(
        src_ref=nrm.at[other], dst_ref=peer_out, send_sem=nrm_sem.at[0], recv_sem=nrm_sem.at[1],
        device_id={"tp": other}, device_id_type=MESH,
    )
    nrm_copy.start()
    own_out[...] = nrm[tp]
    nrm_copy.wait()
    for d in range(1, KVN):
        to = lax.rem(kv + d, KVN)
        total_copy(to, kv).wait_send()
        state_copy(to, kv).wait_send()
        back_copy(to, kv).wait_send()


def finish_kernel(own, peer, w_out, prompt_in, dec_key, dec_value, dec_decay, decode_state, mixed, mixed_dec, prompt_out, dec_out, lhs):
    tp = lax.axis_index("tp")
    n = pl.program_id(0)
    half_width = own.shape[-1]

    @pl.when(n == 0)
    def _():
        order = order_matrix()
        prompt_out[...] = prompt_in[...]
        for src, at in ((own, tp), (peer, 1 - tp)):
            cols = pl.ds(pl.multiple_of(at * half_width, half_width), half_width)
            lhs[:RP, cols] = dotg(order, src[:RP], TN).astype(BF16)
            lhs[RP:, cols] = src[RP:]

    got = dot(lhs[...], w_out[...]).astype(BF16)
    mixed[...] = got[:RP].reshape(OWN, PR, got.shape[-1])
    mixed_dec[...] = got[RP : RP + 2]
    row = lax.broadcasted_iota(jnp.int32, (PAD, 1), 0)
    for e in range(2):
        idx = 2 * n + e
        token, h = idx // HEADS, idx % HEADS
        half, r = token // 2, token % 2
        key = jnp.where(row == r, dec_key[half, h].astype(F32), 0.0).astype(BF16)
        fresh = dotg(key, dec_value[half, h], TN)
        lane = lax.broadcasted_iota(jnp.int32, (1, DK), 1)
        decay = jnp.sum(jnp.where(lane == idx, dec_decay[...], 0.0), axis=-1, keepdims=True)
        dec_out[e] = decay * decode_state[e] + fresh


def on_device(
    pieces, new_tokens, w_query, w_key, w_value, w_decay, decay_bias, norm_gain, head_gain, w_out, prompt_state, decode_state
):
    width = pieces.shape[-1]
    any_spec = pl.BlockSpec(memory_space=pl.ANY)
    vmem = pl.BlockSpec(memory_space=pltpu.VMEM)
    dma = pltpu.SemaphoreType.DMA
    row_k = DK // KVN
    own, peer, prompt_new, dec_key, dec_value, dec_decay = pl.pallas_call(
        attend_kernel,
        name="attend",
        out_shape=(
            jax.ShapeDtypeStruct((ROWS, HEADS * DV), BF16),
            jax.ShapeDtypeStruct((ROWS, HEADS * DV), BF16),
            jax.ShapeDtypeStruct((PH, row_k, DV), F32),
            jax.ShapeDtypeStruct((2, HEADS, PAD, DK), BF16),
            jax.ShapeDtypeStruct((2, HEADS, PAD, DV), BF16),
            jax.ShapeDtypeStruct((DK, DK), F32),
        ),
        in_specs=[any_spec] * 11,
        out_specs=(vmem,) * 6,
        scratch_shapes=[
            pltpu.VMEM((OWN, PR, width), BF16),
            pltpu.VMEM((2, width), BF16),
            pltpu.VMEM((width, HEADS * DK), BF16),
            pltpu.VMEM((width, HEADS * DK), BF16),
            pltpu.VMEM((width, HEADS * DV), BF16),
            pltpu.VMEM((width, HEADS * DK), BF16),
            pltpu.VMEM((1, 2 * HEADS * DK), F32),
            pltpu.VMEM((1, width), F32),
            pltpu.VMEM((1, width), F32),
            pltpu.VMEM((PH, row_k, DV), F32),
            pltpu.VMEM((4, HEADS, DK, DV), F32),
            pltpu.VMEM((RP, width), F32),
            pltpu.VMEM((2, ROWS, width), BF16),
            pltpu.VMEM((HEADS, 2, ROWS, DK), BF16),
            pltpu.VMEM((HEADS, 2, ROWS, DK), BF16),
            pltpu.VMEM((HEADS, 2, ROWS, DV), BF16),
            pltpu.VMEM((HEADS, 2, ROWS, DK), F32),
            pltpu.VMEM((HEADS, 2, PR, OWN, DK), F32),
            pltpu.VMEM((KVN, PH, row_k, DV), BF16),
            pltpu.VMEM((DK, DK), F32),
            pltpu.VMEM((KVN, row_k, DK), F32),
            pltpu.VMEM((KVN, PH, row_k, DV), BF16),
            pltpu.VMEM((KVN, row_k, DK), F32),
            pltpu.VMEM((KVN, PH, row_k, DV), BF16),
            pltpu.VMEM((KVN, PH, row_k, DV), BF16),
            pltpu.VMEM((PH, 2, OWN, DV), F32),
            pltpu.VMEM((PH, 2, OWN, DK), BF16),
            pltpu.VMEM((2, ROWS, HEADS * DV), BF16),
            dma((11,)),
            dma((2,)),
            dma((KVN,)),
            dma((KVN,)),
            dma((KVN,)),
            dma((KVN,)),
            dma((KVN,)),
            dma((KVN,)),
            dma((2,)),
        ],
        compiler_params=pltpu.CompilerParams(collective_id=0, has_side_effects=True, vmem_limit_bytes=44 * 1024 * 1024),
    )(
        pieces, new_tokens, w_query, w_key, w_value, w_decay, decay_bias.reshape(1, -1), norm_gain.reshape(1, -1),
        head_gain.reshape(1, -1), prompt_state.reshape(PH, row_k, DV), decode_state,
    )
    steps = 8
    tile = width // steps
    full = lambda *shape: pl.BlockSpec(shape, lambda n: (0,) * len(shape))
    mixed, mixed_dec, prompt_out, dec_out = pl.pallas_call(
        finish_kernel,
        name="finish",
        grid=(steps,),
        out_shape=(
            jax.ShapeDtypeStruct((OWN, PR, width), BF16),
            jax.ShapeDtypeStruct((2, width), BF16),
            jax.ShapeDtypeStruct((PH, row_k, DV), F32),
            jax.ShapeDtypeStruct((4 * HEADS, DK, DV), F32),
        ),
        in_specs=[
            full(ROWS, HEADS * DV),
            full(ROWS, HEADS * DV),
            pl.BlockSpec((width, tile), lambda n: (0, n)),
            full(PH, row_k, DV),
            full(2, HEADS, PAD, DK),
            full(2, HEADS, PAD, DV),
            full(DK, DK),
            pl.BlockSpec((2, DK, DV), lambda n: (n, 0, 0)),
        ],
        out_specs=(
            pl.BlockSpec((OWN, PR, tile), lambda n: (0, 0, n)),
            pl.BlockSpec((2, tile), lambda n: (0, n)),
            full(PH, row_k, DV),
            pl.BlockSpec((2, DK, DV), lambda n: (n, 0, 0)),
        ),
        scratch_shapes=[pltpu.VMEM((ROWS, width), BF16)],
        compiler_params=pltpu.CompilerParams(dimension_semantics=("arbitrary",), vmem_limit_bytes=32 * 1024 * 1024),
    )(own, peer, w_out, prompt_new, dec_key, dec_value, dec_decay, decode_state.reshape(4 * HEADS, DK, DV))
    return (
        mixed,
        mixed_dec,
        prompt_out.reshape(prompt_state.shape),
        dec_out.reshape(decode_state.shape),
    )


def solution(mesh):
    kv_tp, dp_kv_tp = ("kv", "tp"), ("dp", "kv", "tp")
    return jax.shard_map(
        on_device,
        mesh=mesh,
        in_specs=(
            P(kv_tp, "dp", None),
            P(dp_kv_tp, None),
            P(None, "tp"),
            P(None, "tp"),
            P(None, "tp"),
            P(None, "tp"),
            P(),
            P(),
            P(),
            P(),
            P("dp", "tp", "kv", None),
            P(("dp", "kv"), "tp", None, None),
        ),
        out_specs=(
            P(kv_tp, "dp", None),
            P(dp_kv_tp, None),
            P("dp", "tp", "kv", None),
            P(("dp", "kv"), "tp", None, None),
        ),
        check_vma=False,
    )
```

time: 269 us -> 56.1 us (0.21)
  waiting for transfers between devices: 67.7 us -> 0 us
  local copies, waits for them, and re-layouts: 67 us -> 9.61 us
  other arithmetic: 50.6 us -> 0 us
  Pallas kernels: 0 us -> 45.4 us
  blocking collectives: 25.7 us -> 0 us
  starting transfers between devices: 22.6 us -> 0 us
  matrix products: 18.5 us -> 0 us
  between operations: 14.5 us -> 0.68 us
    all_gather x2 -> x0, waiting for transfers between devices: 48.9 us -> none  [entering(): pieces = jax.tree.map(lambda part: lax.all_gather(part, axis), subtotal)]
    pallas_call x0 -> x2, Pallas kernels: none -> 45.4 us  [the longest x1 38.5 us: on_device(): pl.pallas_call(attend_kernel, name='attend', out_shape=(jax.ShapeDtypeStr...]
    convert_element_type x19 -> x0, other arithmetic: 22.8 us -> none  [the longest x1 4.79 us: split_roles(): queries = (product[..., :qk_cols] * DK ** (-0.5)).astype(jnp.bfloat16)]
    all_to_all x4 -> x0, starting transfers between devices: 22.6 us -> none  [the longest x3 16.5 us: copy_for_each(): return lax.all_to_all(copies, axis, split_axis=0, concat_axis=0, tiled=True)]
    all_gather x2 -> x0, blocking collectives: 20.4 us -> none  [entering(): pieces = jax.tree.map(lambda part: lax.all_gather(part, axis), subtotal)]
    reshape x7 -> x0, local copies, waits for them, and re-layouts: 20 us -> none  [the longest x1 7.42 us: on_device(): products[:, :piece_count]]
    all_to_all x4 -> x0, waiting for transfers between devices: 18.8 us -> none  [the longest x3 9.95 us: copy_for_each(): return lax.all_to_all(copies, axis, split_axis=0, concat_axis=0, tiled=True)]
    dot_general x16 -> x0, matrix products: 18.5 us -> none  [the longest x1 3.01 us: on_device(): jnp.dot(row_block, w_decay, preferred_element_type=jnp.float32)]
  transfers between devices with their start and end apart: 6 -> 0, of which waited for: 5 -> 0; matrix products, arithmetic and copies ran while one was open for 3% -> 0% of each run, Pallas kernels for 0% -> 0%
where the time goes in v1:
time: 56.1 us; the launch traced here: 55.6 us
  Pallas kernels  45.4 us (81%)
  local copies, waits for them, and re-layouts  9.61 us (17%)
  between operations  0.68 us (1%)
    pallas_call x1, Pallas kernels, on_device(): pl.pallas_call(attend_kernel, name='attend', out_shape=(jax.ShapeDtypeStr...  38.5 us
    unnamed x22, local copies, waits for them, and re-layouts  9.61 us
    pallas_call x1, Pallas kernels, on_device(): pl.pallas_call(finish_kernel, name='finish', grid=(steps,), out_shape=(ja...  6.84 us

profile of v1, /device:TPU:1, one launch (start us, length us, event | category | flops | bytes accessed | tf_op | source)
XLA Modules:
  0.0 55.6 jit_solution(11757025343047793891)
XLA Ops:
  0.6 0.0 copy-start.2
  0.6 1.6 %copy-done.2 = bf16[2048,512]{1,0:T(8,128)(2,1)S(1)} copy-done((bf16[2048,512]{1,0:T(8,128)(2,1)S(1)}, bf16[2048,512]{1,0:T(8,128)(2,1)}, u32[]{:S(2)}) %copy-start.2) | copy-done | bytes 2097176
  2.2 0.0 copy-start.3
  2.2 1.6 %copy-done.3 = bf16[2048,512]{1,0:T(8,128)(2,1)S(1)} copy-done((bf16[2048,512]{1,0:T(8,128)(2,1)S(1)}, bf16[2048,512]{1,0:T(8,128)(2,1)}, u32[]{:S(2)}) %copy-start.3) | copy-done | bytes 2097176
  3.8 0.0 copy-start.4
  3.8 1.6 %copy-done.4 = bf16[2048,512]{1,0:T(8,128)(2,1)S(1)} copy-done((bf16[2048,512]{1,0:T(8,128)(2,1)S(1)}, bf16[2048,512]{1,0:T(8,128)(2,1)}, u32[]{:S(2)}) %copy-start.4) | copy-done | bytes 2097176
  5.4 0.0 copy-start.5
  5.4 1.2 %copy-done.5 = bf16[128,2,2048]{2,1,0:T(2,128)(2,1)S(1)} copy-done((bf16[128,2,2048]{2,1,0:T(2,128)(2,1)S(1)}, bf16[128,2,2048]{2,1,0:T(2,128)(2,1)}, u32[]{:S(2)}) %copy-start.5) | copy-done | bytes 1048600
  6.6 0.0 copy-start.6
  6.6 0.8 %copy-done.6 = f32[2,4,8,256]{3,2,1,0:T(8,128)S(1)} copy-done((f32[2,4,8,256]{3,2,1,0:T(8,128)S(1)}, f32[2,4,8,256]{3,2,1,0:T(8,128)}, u32[]{:S(2)}) %copy-start.6) | copy-done | bytes 65560
  7.5 0.0 copy-start.7
  7.5 0.7 %copy-done.7 = bf16[2,2048]{1,0:T(2,128)(2,1)S(1)} copy-done((bf16[2,2048]{1,0:T(2,128)(2,1)S(1)}, bf16[2,2048]{1,0:T(2,128)(2,1)}, u32[]{:S(2)}) %copy-start.7) | copy-done | bytes 8216
  8.2 0.0 copy-start.8
  8.2 0.7 %copy-done.8 = f32[2048]{0:T(1024)S(1)} copy-done((f32[2048]{0:T(1024)S(1)}, f32[2048]{0:T(1024)}, u32[]{:S(2)}) %copy-start.8) | copy-done | bytes 8216
  8.9 0.0 copy-start.9
  8.9 0.7 %copy-done.9 = f32[2048]{0:T(1024)S(1)} copy-done((f32[2048]{0:T(1024)S(1)}, f32[2048]{0:T(1024)}, u32[]{:S(2)}) %copy-start.9) | copy-done | bytes 8216
  9.6 0.0 copy-start.10
  9.6 0.7 %copy-done.10 = f32[1024]{0:T(1024)S(1)} copy-done((f32[1024]{0:T(1024)S(1)}, f32[1024]{0:T(1024)}, u32[]{:S(2)}) %copy-start.10) | copy-done | bytes 4120
  10.3 0.0 copy-start
  10.3 0.0 copy-start.1
  10.3 38.5 %attend.1 = (bf16[272,1024]{1,0:T(8,128)(2,1)S(1)}, bf16[272,1024]{1,0:T(8,128)(2,1)S(1)}, f32[8,8,256]{2,1,0:T(8,128)S(1)}, bf16[2,4,16,128]{3,2,1,0:T(8,128)(2...) custom-call(bf16[128,2,2048]{2,1,0:T(2,128)(2,1)S(1)} %copy-done.5, bf16[2,2048]{1,0:T(2,128)(2,1)S(1)} %copy-done.7, ...), custom_call_target="tpu_custom_call" | custom-call | tf_op jit(solution)/shard_map/attend/pallas_call | solution.py:374
  48.8 0.0 copy-done
  48.8 0.0 copy-done.1
  48.8 6.8 %finish.1 = (bf16[128,2,2048]{2,1,0:T(2,128)(2,1)}, bf16[2,2048]{1,0:T(2,128)(2,1)}, f32[8,8,256]{2,1,0:T(8,128)}, f32[16,128,256]{2,1,0:T(8,128)}) custom-call(bf16[272,1024]{1,0:T(8,128)(2,1)S(1)} %get-tuple-element.14.own, bf16[272,1024]{1,0:T(8,128)(2,1)S(1)} %get-tuple-element.15.peer, bf16[2048,2048]{1,0:T(8,128)(2,1)S(1)} %copy-done, ...), custom_call_target="tpu_custom_call" | custom-call | tf_op jit(solution)/shard_map/finish/pallas_call | solution.py:434
Async XLA Ops:
  0.6 1.6 %copy-start.2 = (bf16[2048,512]{1,0:T(8,128)(2,1)S(1)}, bf16[2048,512]{1,0:T(8,128)(2,1)}, u32[]{:S(2)}) copy-start(bf16[2048,512]{1,0:T(8,128)(2,1)} %w_query.1) | copy-start | bytes 6291460
  2.2 1.6 %copy-start.3 = (bf16[2048,512]{1,0:T(8,128)(2,1)S(1)}, bf16[2048,512]{1,0:T(8,128)(2,1)}, u32[]{:S(2)}) copy-start(bf16[2048,512]{1,0:T(8,128)(2,1)} %w_key.1) | copy-start | bytes 6291460
  3.8 1.6 %copy-start.4 = (bf16[2048,512]{1,0:T(8,128)(2,1)S(1)}, bf16[2048,512]{1,0:T(8,128)(2,1)}, u32[]{:S(2)}) copy-start(bf16[2048,512]{1,0:T(8,128)(2,1)} %w_decay.1) | copy-start | bytes 6291460
  5.4 1.2 %copy-start.5 = (bf16[128,2,2048]{2,1,0:T(2,128)(2,1)S(1)}, bf16[128,2,2048]{2,1,0:T(2,128)(2,1)}, u32[]{:S(2)}) copy-start(bf16[128,2,2048]{2,1,0:T(2,128)(2,1)} %pieces.1) | copy-start | bytes 3145732
  6.6 0.8 %copy-start.6 = (f32[2,4,8,256]{3,2,1,0:T(8,128)S(1)}, f32[2,4,8,256]{3,2,1,0:T(8,128)}, u32[]{:S(2)}) copy-start(f32[2,4,8,256]{3,2,1,0:T(8,128)} %param.22) | copy-start | bytes 196612
  7.5 0.7 %copy-start.7 = (bf16[2,2048]{1,0:T(2,128)(2,1)S(1)}, bf16[2,2048]{1,0:T(2,128)(2,1)}, u32[]{:S(2)}) copy-start(bf16[2,2048]{1,0:T(2,128)(2,1)} %new_tokens.1) | copy-start | bytes 24580
  8.2 0.7 %copy-start.8 = (f32[2048]{0:T(1024)S(1)}, f32[2048]{0:T(1024)}, u32[]{:S(2)}) copy-start(f32[2048]{0:T(1024)} %param.19) | copy-start | bytes 24580
  8.9 0.7 %copy-start.9 = (f32[2048]{0:T(1024)S(1)}, f32[2048]{0:T(1024)}, u32[]{:S(2)}) copy-start(f32[2048]{0:T(1024)} %param.20) | copy-start | bytes 24580
  9.6 0.7 %copy-start.10 = (f32[1024]{0:T(1024)S(1)}, f32[1024]{0:T(1024)}, u32[]{:S(2)}) copy-start(f32[1024]{0:T(1024)} %param.18) | copy-start | bytes 12292
  10.3 38.5 %copy-start = (bf16[2048,2048]{1,0:T(8,128)(2,1)S(1)}, bf16[2048,2048]{1,0:T(8,128)(2,1)}, u32[]{:S(2)}) copy-start(bf16[2048,2048]{1,0:T(8,128)(2,1)} %w_out.1) | copy-start | bytes 25165828
  10.3 38.5 %copy-start.1 = (f32[4,4,128,256]{3,2,1,0:T(8,128)S(1)}, f32[4,4,128,256]{3,2,1,0:T(8,128)}, u32[]{:S(2)}) copy-start(f32[4,4,128,256]{3,2,1,0:T(8,128)} %decode_state.1) | copy-start | bytes 6291460

commit v2 on v1

--- a/solution.py
+++ b/solution.py
@@ -50,7 +50,7 @@
 
 def attend_kernel(
     pieces, new_tokens, w_query, w_key, w_value, w_decay, bias, gain, head_gain, prompt_state, decode_state,
-    own_out, peer_out, prompt_out, dec_key, dec_value, dec_decay,
+    own_out, peer_out, prompt_out, dec_new,
     x3, nt, wq, wk, wv, wd, bias_v, gain_v, hg_v, ps, ds, xs, rows, qb, kb, vb, db, bb, st, tt, ttt, rs, rt, sb, inc, att,
     sqc, nrm, load_sem, row_sem, st_send, st_recv, tt_send, tt_recv, in_send, in_recv, nrm_sem,
 ):
@@ -281,9 +281,15 @@
                 out = out + jnp.where(row == r, from_state, 0.0)
                 tt[pl.ds((each * half + r) * HEADS + h, 1), :] = eg[r : r + 1]
             nrm[half, RP:, h * DV : (h + 1) * DV] = normed(out, h)
-            dec_key[half, h] = kb[h, half, RP:]
-            dec_value[half, h] = vb[h, half, RP:]
-    dec_decay[...] = tt[...].T
+    tt[...] = tt[...].T
+    for half in range(2):
+        for h in range(HEADS):
+            for r in range(each):
+                token = each * half + r
+                key = jnp.where(row == r, kb[h, half, RP:].astype(F32), 0.0).astype(BF16)
+                fresh = dotg(key, vb[h, half, RP:], TN)
+                idx = token * HEADS + h
+                dec_new[token, h] = tt[:, idx : idx + 1] * ds[token, h] + fresh
 
     def scan_step(i, state):
         @pl.when(i != kv)
@@ -334,56 +340,61 @@
         back_copy(to, kv).wait_send()
 
 
-def finish_kernel(own, peer, w_out, prompt_in, dec_key, dec_value, dec_decay, decode_state, mixed, mixed_dec, prompt_out, dec_out, lhs):
+def finish_kernel(own, peer, w_out, prompt_in, dec_in, mixed, mixed_dec, prompt_out, dec_out, lhs, out3, out2, sem, tile_sem):
     tp = lax.axis_index("tp")
-    n = pl.program_id(0)
     half_width = own.shape[-1]
-
-    @pl.when(n == 0)
-    def _():
-        order = order_matrix()
-        prompt_out[...] = prompt_in[...]
-        for src, at in ((own, tp), (peer, 1 - tp)):
-            cols = pl.ds(pl.multiple_of(at * half_width, half_width), half_width)
-            lhs[:RP, cols] = dotg(order, src[:RP], TN).astype(BF16)
-            lhs[RP:, cols] = src[RP:]
-
-    got = dot(lhs[...], w_out[...]).astype(BF16)
-    mixed[...] = got[:RP].reshape(OWN, PR, got.shape[-1])
-    mixed_dec[...] = got[RP : RP + 2]
-    row = lax.broadcasted_iota(jnp.int32, (PAD, 1), 0)
-    for e in range(2):
-        idx = 2 * n + e
-        token, h = idx // HEADS, idx % HEADS
-        half, r = token // 2, token % 2
-        key = jnp.where(row == r, dec_key[half, h].astype(F32), 0.0).astype(BF16)
-        fresh = dotg(key, dec_value[half, h], TN)
-        lane = lax.broadcasted_iota(jnp.int32, (1, DK), 1)
-        decay = jnp.sum(jnp.where(lane == idx, dec_decay[...], 0.0), axis=-1, keepdims=True)
-        dec_out[e] = decay * decode_state[e] + fresh
+    width = w_out.shape[-1]
+    copies = [pltpu.make_async_copy(dec_in, dec_out, sem.at[0]), pltpu.make_async_copy(prompt_in, prompt_out, sem.at[1])]
+    for copy in copies:
+        copy.start()
+    order = order_matrix()
+    for src, at in ((own, tp), (peer, 1 - tp)):
+        cols = pl.ds(pl.multiple_of(at * half_width, half_width), half_width)
+        lhs[:RP, cols] = dotg(order, src[:RP], TN).astype(BF16)
+        lhs[RP:, cols] = src[RP:]
+    tile = 256
+
+    def out_copy(n):
+        cols = pl.ds(pl.multiple_of(n * tile, tile), tile)
+        return pltpu.make_async_copy(out3.at[:, :, cols], mixed.at[:, :, cols], tile_sem.at[n])
+
+    def body(n, _):
+        cols = pl.ds(pl.multiple_of(n * tile, tile), tile)
+        got = dot(lhs[...], w_out[:, cols]).astype(BF16)
+        out3[:, :, cols] = got[:RP].reshape(OWN, PR, tile)
+        out2[:, cols] = got[RP : RP + 2]
+        out_copy(n).start()
+        return 0
+
+    lax.fori_loop(0, width // tile, body, 0)
+    last = pltpu.make_async_copy(out2, mixed_dec, sem.at[2])
+    last.start()
+    for n in range(width // tile):
+        out_copy(n).wait()
+    last.wait()
+    for copy in copies:
+        copy.wait()
 
 
 def on_device(
     pieces, new_tokens, w_query, w_key, w_value, w_decay, decay_bias, norm_gain, head_gain, w_out, prompt_state, decode_state
 ):
     width = pieces.shape[-1]
-    any_spec = pl.BlockSpec(memory_space=pl.ANY)
     vmem = pl.BlockSpec(memory_space=pltpu.VMEM)
     dma = pltpu.SemaphoreType.DMA
     row_k = DK // KVN
-    own, peer, prompt_new, dec_key, dec_value, dec_decay = pl.pallas_call(
+    hbm = pl.BlockSpec(memory_space=pltpu.HBM)
+    own, peer, prompt_new, dec_new = pl.pallas_call(
         attend_kernel,
         name="attend",
         out_shape=(
             jax.ShapeDtypeStruct((ROWS, HEADS * DV), BF16),
             jax.ShapeDtypeStruct((ROWS, HEADS * DV), BF16),
             jax.ShapeDtypeStruct((PH, row_k, DV), F32),
-            jax.ShapeDtypeStruct((2, HEADS, PAD, DK), BF16),
-            jax.ShapeDtypeStruct((2, HEADS, PAD, DV), BF16),
-            jax.ShapeDtypeStruct((DK, DK), F32),
+            jax.ShapeDtypeStruct((4, HEADS, DK, DV), F32),
         ),
-        in_specs=[any_spec] * 11,
-        out_specs=(vmem,) * 6,
+        in_specs=[hbm] * 11,
+        out_specs=(vmem,) * 4,
         scratch_shapes=[
             pltpu.VMEM((OWN, PR, width), BF16),
             pltpu.VMEM((2, width), BF16),
@@ -425,46 +436,39 @@
         ],
         compiler_params=pltpu.CompilerParams(collective_id=0, has_side_effects=True, vmem_limit_bytes=44 * 1024 * 1024),
     )(
-        pieces, new_tokens, w_query, w_key, w_value, w_decay, decay_bias.reshape(1, -1), norm_gain.reshape(1, -1),
-        head_gain.reshape(1, -1), prompt_state.reshape(PH, row_k, DV), decode_state,
+        *(
+            pltpu.with_memory_space_constraint(a, pltpu.HBM)
+            for a in (
+                pieces, new_tokens, w_query, w_key, w_value, w_decay, decay_bias.reshape(1, -1), norm_gain.reshape(1, -1),
+                head_gain.reshape(1, -1), prompt_state.reshape(PH, row_k, DV), decode_state,
+            )
+        )
     )
-    steps = 8
-    tile = width // steps
-    full = lambda *shape: pl.BlockSpec(shape, lambda n: (0,) * len(shape))
     mixed, mixed_dec, prompt_out, dec_out = pl.pallas_call(
         finish_kernel,
         name="finish",
-        grid=(steps,),
         out_shape=(
             jax.ShapeDtypeStruct((OWN, PR, width), BF16),
             jax.ShapeDtypeStruct((2, width), BF16),
             jax.ShapeDtypeStruct((PH, row_k, DV), F32),
-            jax.ShapeDtypeStruct((4 * HEADS, DK, DV), F32),
+            jax.ShapeDtypeStruct((4, HEADS, DK, DV), F32),
         ),
-        in_specs=[
-            full(ROWS, HEADS * DV),
-            full(ROWS, HEADS * DV),
-            pl.BlockSpec((width, tile), lambda n: (0, n)),
-            full(PH, row_k, DV),
-            full(2, HEADS, PAD, DK),
-            full(2, HEADS, PAD, DV),
-            full(DK, DK),
-            pl.BlockSpec((2, DK, DV), lambda n: (n, 0, 0)),
+        in_specs=[vmem] * 5,
+        out_specs=(hbm,) * 4,
+        scratch_shapes=[
+            pltpu.VMEM((ROWS, width), BF16),
+            pltpu.VMEM((OWN, PR, width), BF16),
+            pltpu.VMEM((2, width), BF16),
+            dma((3,)),
+            dma((width // 256,)),
         ],
-        out_specs=(
-            pl.BlockSpec((OWN, PR, tile), lambda n: (0, 0, n)),
-            pl.BlockSpec((2, tile), lambda n: (0, n)),
-            full(PH, row_k, DV),
-            pl.BlockSpec((2, DK, DV), lambda n: (n, 0, 0)),
-        ),
-        scratch_shapes=[pltpu.VMEM((ROWS, width), BF16)],
-        compiler_params=pltpu.CompilerParams(dimension_semantics=("arbitrary",), vmem_limit_bytes=32 * 1024 * 1024),
-    )(own, peer, w_out, prompt_new, dec_key, dec_value, dec_decay, decode_state.reshape(4 * HEADS, DK, DV))
+        compiler_params=pltpu.CompilerParams(vmem_limit_bytes=32 * 1024 * 1024),
+    )(own, peer, w_out, prompt_new, dec_new)
     return (
         mixed,
         mixed_dec,
         prompt_out.reshape(prompt_state.shape),
-        dec_out.reshape(decode_state.shape),
+        dec_out,
     )
 
 

time: 56.1 us -> 45.3 us (0.81)
  local copies, waits for them, and re-layouts: 9.61 us -> 0.01 us
  Pallas kernels: 45.4 us -> 44.5 us
    unnamed x22 -> x2, local copies, waits for them, and re-layouts: 9.61 us -> 0.01 us
    pallas_call x1, Pallas kernels: 6.84 us -> 5.14 us  [on_device(): pl.pallas_call(finish_kernel, name='finish', out_shape=(jax.ShapeDtypeStr...]
    pallas_call x1, Pallas kernels: 38.5 us -> 39.4 us  [on_device(): pl.pallas_call(attend_kernel, name='attend', out_shape=(jax.ShapeDtypeStr...]
where the time goes in v2:
time: 45.3 us; the launch traced here: 45.2 us
  Pallas kernels  44.5 us (98%)
  between operations  0.66 us (1%)
    pallas_call x1, Pallas kernels, on_device(): pl.pallas_call(attend_kernel, name='attend', out_shape=(jax.ShapeDtypeStr...  39.4 us
    pallas_call x1, Pallas kernels, on_device(): pl.pallas_call(finish_kernel, name='finish', out_shape=(jax.ShapeDtypeStr...  5.14 us

profile of v2, /device:TPU:1, one launch (start us, length us, event | category | flops | bytes accessed | tf_op | source)
XLA Modules:
  0.0 45.2 jit_solution(12346878288677815774)
XLA Ops:
  0.6 0.0 copy-start
  0.6 39.4 %attend.1 = (bf16[272,1024]{1,0:T(8,128)(2,1)S(1)}, bf16[272,1024]{1,0:T(8,128)(2,1)S(1)}, f32[8,8,256]{2,1,0:T(8,128)S(1)}, f32[4,4,128,256]{3,2,1,0:T(8,128)S(1)}) custom-call(bf16[128,2,2048]{2,1,0:T(2,128)(2,1)} %pieces.1, bf16[2,2048]{1,0:T(2,128)(2,1)} %new_tokens.1, bf16[2048,512]{1,0:T(8,128)(2,1)} %w_query.1, bf16[2048,512]{1,0:T(8,128)(2,1)} %w_key.1, ...), custom_call_target="tpu_custom_call" | custom-call | tf_op jit(solution)/shard_map/attend/pallas_call | solution.py:387
  40.0 0.0 copy-done
  40.0 5.1 %finish.1 = (bf16[128,2,2048]{2,1,0:T(2,128)(2,1)}, bf16[2,2048]{1,0:T(2,128)(2,1)}, f32[8,8,256]{2,1,0:T(8,128)}, f32[4,4,128,256]{3,2,1,0:T(8,128)}) custom-call(bf16[272,1024]{1,0:T(8,128)(2,1)S(1)} %get-tuple-element.12.own, bf16[272,1024]{1,0:T(8,128)(2,1)S(1)} %get-tuple-element.13.peer, bf16[2048,2048]{1,0:T(8,128)(2,1)S(1)} %copy-done, ...), custom_call_target="tpu_custom_call" | custom-call | tf_op jit(solution)/shard_map/finish/pallas_call | solution.py:447
Async XLA Ops:
  0.6 39.4 %copy-start = (bf16[2048,2048]{1,0:T(8,128)(2,1)S(1)}, bf16[2048,2048]{1,0:T(8,128)(2,1)}, u32[]{:S(2)}) copy-start(bf16[2048,2048]{1,0:T(8,128)(2,1)} %w_out.1) | copy-start | bytes 25165828

commit v3 on v2

v3 whole, which is shorter than its diff:
```python
import functools

import jax
import jax.numpy as jnp
from jax import lax
from jax.experimental import pallas as pl
from jax.experimental.pallas import tpu as pltpu
from jax.sharding import PartitionSpec as P

F32 = jnp.float32
BF16 = jnp.bfloat16
MESH = pl.DeviceIdType.MESH

DK = 128
DV = 256
EPS = 0.1
TAU = 16.0
SUB = 16
BLK = 64
HEADS = 4
PR = 2
OWN = 128
PAD = 16
RP = PR * OWN
ROWS = RP + PAD
KVN = 16
SIDE = 4
ROW_K = DK // KVN
PH = PR * HEADS
TN = (((0,), (0,)), ((), ()))
NT = (((1,), (1,)), ((), ()))


def dot(a, b):
    return jnp.dot(a, b, preferred_element_type=F32)


def dotg(a, b, dims):
    return lax.dot_general(a, b, dims, preferred_element_type=F32)


def log_decay(x):
    return (jnp.minimum(x, 0.0) - jnp.log1p(jnp.exp(-jnp.abs(x)))) / TAU


def order_matrix():
    m = lax.broadcasted_iota(jnp.int32, (RP, RP), 0)
    n = lax.broadcasted_iota(jnp.int32, (RP, RP), 1)
    first = jnp.where(m < OWN, PR * m, PR * (m - OWN) + 1)
    return jnp.where(n == first, 1.0, 0.0).astype(BF16)


def by_distance():
    offsets = [(dz, dy) for dz in range(SIDE) for dy in range(SIDE) if dz or dy]
    return sorted(offsets, key=lambda o: -min(o[0], SIDE - o[0]) - min(o[1], SIDE - o[1]))


def attend_kernel(
    pieces, new_tokens, w_query, w_key, w_value, w_decay, bias, gain, head_gain, prompt_state, decode_state, w_out,
    acc, peer, w_last, prompt_out, dec_new,
    x3, nt, wq, wk, wv, wd, bias_v, gain_v, hg_v, ps, ds, wo, xs, rows, qb, kb, vb, db, bb, st, tt, ttt, rs, rt, sb, inc,
    att, sqc, nrm, peer0, load_sem, wo_sem, row_sem, st_send, st_recv, tt_send, tt_recv, in_send, in_recv, nrm_sem,
):
    kv = lax.axis_index("kv")
    tp = lax.axis_index("tp")
    other = 1 - tp
    width = rows.shape[-1]

    def load(i, src, dst):
        return pltpu.make_async_copy(src, dst, load_sem.at[i])

    load_x = load(0, pieces, x3)
    load_nt = load(1, new_tokens, nt)
    load_gain = load(2, gain, gain_v)
    load_d = load(3, w_decay, wd)
    load_k = load(4, w_key, wk)
    load_v = load(5, w_value, wv)
    load_bias = load(6, bias, bias_v)
    load_q = load(7, w_query, wq)
    load_ps = load(8, prompt_state, ps)
    load_ds = load(9, decode_state, ds)
    load_hg = load(10, head_gain, hg_v)
    for copy in (load_x, load_nt, load_gain, load_bias, load_d):
        copy.start()

    barrier = pltpu.get_barrier_semaphore()
    pl.semaphore_signal(barrier, inc=1, device_id={"tp": other}, device_id_type=MESH)
    z, y = kv // SIDE, kv % SIDE
    peers = [lax.rem(z + dz, SIDE) * SIDE + lax.rem(y + dy, SIDE) for dz, dy in by_distance()]
    for to in peers:
        pl.semaphore_signal(barrier, inc=1, device_id={"kv": to}, device_id_type=MESH)

    order = order_matrix()
    for copy in (load_x, load_nt, load_gain):
        copy.wait()
    for copy in (load_k, load_v):
        copy.start()
    flat = x3[...].reshape(RP, width)
    step = 512
    squares = jnp.zeros((RP, 1), F32)
    for c in range(width // step):
        part = dot(order, flat[:, c * step : (c + 1) * step])
        xs[:, c * step : (c + 1) * step] = part
        squares += jnp.sum(part * part, axis=-1, keepdims=True)
    factor = lax.rsqrt(squares / width + EPS)
    for c in range(width // step):
        cols = slice(c * step, (c + 1) * step)
        rows[tp, :RP, cols] = (xs[:, cols] * factor * gain_v[:, cols]).astype(BF16)
    wide = nt[...].astype(F32)
    nt_factor = lax.rsqrt(jnp.sum(wide * wide, axis=-1, keepdims=True) / width + EPS)
    nt_rows = wide * nt_factor * gain_v[...]
    rows[tp, RP:, :] = jnp.concatenate([nt_rows, jnp.zeros((PAD - nt_rows.shape[0], width), F32)], axis=0).astype(BF16)

    pl.semaphore_wait(barrier, KVN)
    row_copy = pltpu.make_async_remote_copy(
        src_ref=rows.at[tp], dst_ref=rows.at[tp], send_sem=row_sem.at[0], recv_sem=row_sem.at[1],
        device_id={"tp": other}, device_id_type=MESH,
    )
    row_copy.start()
    for copy in (load_q, load_ds, load_ps, load_hg):
        copy.start()

    def project(half, weights, out, kind, first, count):
        per = 2 * DK

        def tile(j, _):
            cols = pl.ds(pl.multiple_of(j * per, per), per)
            got = dot(rows[half], weights[:, cols])
            if kind == "v":
                out[j, half] = got.astype(BF16)
            else:
                for e in range(2):
                    part = got[:, e * DK : (e + 1) * DK]
                    if kind == "q":
                        part = (part * DK**-0.5).astype(BF16)
                    elif kind == "k":
                        part = part.astype(BF16)
                    else:
                        at = pl.multiple_of(tp * (HEADS * DK) + j * per + e * DK, DK)
                        part = log_decay(part + bias_v[:, pl.ds(at, DK)])
                    out[2 * j + e, half] = part
            return 0

        lax.fori_loop(first, first + count, tile, 0)

    load_bias.wait()
    load_d.wait()
    project(tp, wd, db, "d", 0, 2)
    load_k.wait()
    project(tp, wk, kb, "k", 0, 2)
    load_v.wait()
    project(tp, wv, vb, "v", 0, 4)
    row_copy.wait()
    project(other, wd, db, "d", 0, 2)

    t_at = lax.broadcasted_iota(jnp.int32, (OWN, OWN), 0)
    s_at = lax.broadcasted_iota(jnp.int32, (OWN, OWN), 1)
    lower = jnp.where(t_at >= s_at, 1.0, 0.0).astype(BF16)
    lower2 = jnp.concatenate([lower, lower], axis=1)
    tt[...] = jnp.zeros_like(tt)

    for p in range(PR):
        total = jnp.zeros((1, HEADS * DK), F32)
        for half in range(2):
            g = jnp.concatenate([db[h, half, p * OWN : (p + 1) * OWN] for h in range(HEADS)], axis=1)
            hi = g.astype(BF16)
            lo = (g - hi.astype(F32)).astype(BF16)
            got = dot(lower2, jnp.concatenate([hi, lo], axis=0))
            total = total + got[OWN - 1 :]
            for h in range(HEADS):
                bb[h, half, p] = got[:, h * DK : (h + 1) * DK]
        for h in range(HEADS):
            n = (h // 2) * 4 + p * 2 + h % 2
            tt[n : n + 1, :] = total[:, h * DK : (h + 1) * DK]
    ttt[...] = tt[...].T.reshape(KVN, ROW_K, DK)

    def total_copy(to, slot):
        return pltpu.make_async_remote_copy(
            src_ref=ttt.at[to], dst_ref=rt.at[slot], send_sem=tt_send.at[to], recv_sem=tt_recv.at[slot],
            device_id={"kv": to}, device_id_type=MESH,
        )

    def state_copy(s, to, slot):
        return pltpu.make_async_remote_copy(
            src_ref=st.at[s, to], dst_ref=rs.at[s, slot], send_sem=st_send.at[s, to], recv_sem=st_recv.at[s, slot],
            device_id={"kv": to}, device_id_type=MESH,
        )

    def back_copy(s, to, slot):
        return pltpu.make_async_remote_copy(
            src_ref=sb.at[s, to], dst_ref=inc.at[s, slot], send_sem=in_send.at[s, to], recv_sem=in_recv.at[s, slot],
            device_id={"kv": to}, device_id_type=MESH,
        )

    for to in peers:
        total_copy(to, kv).start()
    rt[kv] = ttt[kv]

    for s in range(2):
        project(other, wk, kb, "k", s, 1)
        project(other, wv, vb, "v", 2 * s, 2)
        for p in range(PR):
            at = slice(p * OWN, (p + 1) * OWN)
            for e in range(2):
                h = 2 * s + e
                b0, b1 = bb[h, 0, p], bb[h, 1, p]
                t0, t1 = b0[OWN - 1 :], b1[OWN - 1 :]
                e0 = kb[h, 0, at].astype(F32) * jnp.exp((t0 - b0) + t1)
                e1 = kb[h, 1, at].astype(F32) * jnp.exp(t1 - b1)
                keys = jnp.concatenate([e0.astype(BF16), e1.astype(BF16)], axis=0)
                vals = jnp.concatenate([vb[h, 0, at], vb[h, 1, at]], axis=0)
                state = dotg(keys, vals, TN)
                st[s, :, p * 2 + e] = state.reshape(KVN, ROW_K, DV).astype(BF16)
        for to in peers:
            state_copy(s, to, kv).start()
        rs[s, kv] = st[s, kv]

    quarter = width // 4

    def out_rows(i):
        owner = tp if i < 2 else other
        return w_out.at[pl.ds(pl.multiple_of((2 * owner + i % 2) * quarter, quarter), quarter)]

    out_loads = [pltpu.make_async_copy(out_rows(i), wo.at[i] if i < 3 else w_last, wo_sem.at[i]) for i in range(4)]
    for copy in out_loads:
        copy.start()
    load_q.wait()
    project(0, wq, qb, "q", 0, 2)
    project(1, wq, qb, "q", 0, 2)

    t_in = lax.broadcasted_iota(jnp.int32, (BLK, BLK), 0)
    s_in = lax.broadcasted_iota(jnp.int32, (BLK, BLK), 1)
    keep = t_in >= s_in

    def inside(i, _):
        p, h = (i // 2) % 2, 2 * (i // 4) + i % 2
        at = pl.ds(pl.multiple_of(p * OWN, OWN), OWN)
        ks = [kb[h, half, at].astype(F32) for half in range(2)]
        qs = [qb[h, half, at].astype(F32) for half in range(2)]
        bs = [bb[h, half, p] for half in range(2)]
        vs = [vb[h, half, at] for half in range(2)]
        m0, t0 = bs[0][BLK - 1 : BLK], bs[0][OWN - 1 :]
        m1 = bs[1][BLK - 1 : BLK]
        first = (ks[0][:BLK] * jnp.exp(m0 - bs[0][:BLK])).astype(BF16)
        state1 = dotg(first, vs[0][:BLK], TN)
        second = ks[0] * jnp.exp(t0 - bs[0])
        state2 = dotg(second.astype(BF16), vs[0], TN)
        third = jnp.concatenate(
            [(ks[0] * jnp.exp((t0 - bs[0]) + m1)).astype(BF16), (ks[1][:BLK] * jnp.exp(m1 - bs[1][:BLK])).astype(BF16)], axis=0
        )
        state3 = dotg(third, jnp.concatenate([vs[0], vs[1][:BLK]], axis=0), TN)
        starts = [None, state1, state2, state3]
        for blk in range(4):
            half, lo = blk // 2, (blk % 2) * BLK
            b = bs[half][lo : lo + BLK]
            q = qs[half][lo : lo + BLK]
            k = ks[half][lo : lo + BLK]
            v = vs[half][lo : lo + BLK]
            ref = [jnp.zeros((1, DK), F32) if lo == 0 else bs[half][lo - 1 : lo]]
            for n in range(1, BLK // SUB):
                ref.append(b[n * SUB - 1 : n * SUB])
            zero = jnp.zeros((SUB, DK), BF16)
            q_rows, k_cols = [], []
            for n in range(BLK // SUB):
                end = (n + 1) * SUB
                near_q = (q[n * SUB : end] * jnp.exp(b[n * SUB : end] - ref[n])).astype(BF16)
                near_k = (k[:end] * jnp.exp(ref[n] - b[:end])).astype(BF16)
                q_rows.append(jnp.concatenate([near_q if m == n else zero for m in range(BLK // SUB)], axis=1))
                k_cols.append(jnp.concatenate([near_k] + [zero] * (BLK // SUB - 1 - n), axis=0))
            scores = dotg(jnp.concatenate(q_rows, axis=0), jnp.concatenate(k_cols, axis=1), NT)
            weights = jnp.where(keep, scores, 0.0).astype(BF16)
            if blk == 0:
                out = dot(weights, v)
            else:
                start_q = (q * jnp.exp(b - ref[0])).astype(BF16)
                out = dot(
                    jnp.concatenate([start_q, weights], axis=1),
                    jnp.concatenate([starts[blk].astype(BF16), v], axis=0),
                )
            att[i, half, lo : lo + BLK] = out
        sqc[i, 0] = (qs[0] * jnp.exp(bs[0])).astype(BF16)
        sqc[i, 1] = (qs[1] * jnp.exp(bs[1] + t0)).astype(BF16)
        return 0

    lax.fori_loop(0, PH, inside, 0)

    for copy in (load_ps, load_ds, load_hg):
        copy.wait()

    def normed(out, h):
        scale = lax.rsqrt(jnp.sum(out * out, axis=-1, keepdims=True) / DV + EPS)
        gain_at = pl.multiple_of(tp * (HEADS * DV) + h * DV, DV)
        return (out * scale * hg_v[:, pl.ds(gain_at, DV)]).astype(BF16)

    each = 2
    row = lax.broadcasted_iota(jnp.int32, (PAD, 1), 0)
    tt[...] = jnp.zeros_like(tt)
    for half in range(2):
        for h in range(HEADS):
            q = qb[h, half, RP:].astype(F32)
            k = kb[h, half, RP:].astype(F32)
            v = vb[h, half, RP:].astype(F32)
            eg = jnp.exp(db[h, half, RP:])
            eq = (q * eg).astype(BF16)
            out = jnp.sum(q * k, axis=-1, keepdims=True) * v
            for r in range(each):
                from_state = dot(eq, ds[each * half + r, h].astype(BF16))
                out = out + jnp.where(row == r, from_state, 0.0)
                n = (each * half + r) * HEADS + h
                tt[n : n + 1, :] = eg[r : r + 1]
            nrm[half, h // 2, RP:, (h % 2) * DV : (h % 2 + 1) * DV] = normed(out, h)
    columns = tt[...].T
    for half in range(2):
        for h in range(HEADS):
            for r in range(each):
                token = each * half + r
                key = jnp.where(row == r, kb[h, half, RP:].astype(F32), 0.0).astype(BF16)
                fresh = dotg(key, vb[h, half, RP:], TN)
                n = token * HEADS + h
                dec_new[token, h] = columns[:, n : n + 1] * ds[token, h] + fresh

    for to in peers:
        total_copy(to, to).wait_recv()
    for s in range(2):
        for frm in peers:
            state_copy(s, frm, frm).wait_recv()

        def scan_step(i, state):
            decay = jnp.exp(rt[i])
            after = []
            for m in range(4):
                sb[s, i, m] = state[m].astype(BF16)
                after.append(decay[:, s * 4 + m : s * 4 + m + 1] * state[m] + rs[s, i, m].astype(F32))
            return tuple(after)

        at = [(m // 2) * HEADS + 2 * s + m % 2 for m in range(4)]
        last = lax.fori_loop(0, KVN, scan_step, tuple(ps[n] for n in at))
        for to in peers:
            back_copy(s, to, kv).start()
        inc[s, kv] = sb[s, kv]
        for n, state in zip(at, last):
            prompt_out[n] = state

    def nrm_copy(s):
        return pltpu.make_async_remote_copy(
            src_ref=nrm.at[other, s], dst_ref=peer0 if s == 0 else peer, send_sem=nrm_sem.at[s], recv_sem=nrm_sem.at[2 + s],
            device_id={"tp": other}, device_id_type=MESH,
        )

    def add_product(lhs, weights, fresh):
        left = jnp.concatenate([dotg(order, lhs[:RP], TN).astype(BF16), lhs[RP:]], axis=0)
        tile = 256

        def body(n, _):
            cols = pl.ds(pl.multiple_of(n * tile, tile), tile)
            got = dot(left, weights[:, cols])
            acc[:, cols] = got if fresh else acc[:, cols] + got
            return 0

        lax.fori_loop(0, width // tile, body, 0)

    for s in range(2):
        for frm in peers:
            back_copy(s, frm, frm).wait_recv()
        for p in range(PR):
            for e in range(2):
                m = p * 2 + e
                incoming = inc[s, :, m].astype(F32).reshape(DK, DV).astype(BF16)
                for half in range(2):
                    out = att[4 * s + m, half] + dot(sqc[4 * s + m, half], incoming)
                    nrm[half, s, p * OWN : (p + 1) * OWN, e * DV : (e + 1) * DV] = normed(out, 2 * s + e)
        nrm_copy(s).start()
        out_loads[s].wait()
        add_product(nrm[tp, s], wo.at[s], s == 0)
        nrm_copy(s).wait()
        if s == 0:
            out_loads[2].wait()
            add_product(peer0[...], wo.at[2], False)
    out_loads[3].wait()
    for to in peers:
        total_copy(to, kv).wait_send()
        for s in range(2):
            state_copy(s, to, kv).wait_send()
            back_copy(s, to, kv).wait_send()


def finish_kernel(acc, peer, w_last, prompt_in, dec_in, mixed, mixed_dec, prompt_out, dec_out, out3, out2, sem, tile_sem):
    width = acc.shape[-1]
    copies = [pltpu.make_async_copy(dec_in, dec_out, sem.at[0]), pltpu.make_async_copy(prompt_in, prompt_out, sem.at[1])]
    for copy in copies:
        copy.start()
    order = order_matrix()
    left = jnp.concatenate([dotg(order, peer[:RP], TN).astype(BF16), peer[RP:]], axis=0)
    tile = 256

    def out_copy(n):
        cols = pl.ds(pl.multiple_of(n * tile, tile), tile)
        return pltpu.make_async_copy(out3.at[:, :, cols], mixed.at[:, :, cols], tile_sem.at[n])

    def body(n, _):
        cols = pl.ds(pl.multiple_of(n * tile, tile), tile)
        got = (acc[:, cols] + dot(left, w_last[:, cols])).astype(BF16)
        out3[:, :, cols] = got[:RP].reshape(OWN, PR, tile)
        out2[:, cols] = got[RP : RP + 2]
        out_copy(n).start()
        return 0

    lax.fori_loop(0, width // tile, body, 0)
    last = pltpu.make_async_copy(out2, mixed_dec, sem.at[2])
    last.start()
    for n in range(width // tile):
        out_copy(n).wait()
    last.wait()
    for copy in copies:
        copy.wait()


def on_device(
    pieces, new_tokens, w_query, w_key, w_value, w_decay, decay_bias, norm_gain, head_gain, w_out, prompt_state, decode_state
):
    width = pieces.shape[-1]
    vmem = pl.BlockSpec(memory_space=pltpu.VMEM)
    dma = pltpu.SemaphoreType.DMA
    hbm = pl.BlockSpec(memory_space=pltpu.HBM)
    acc, peer, w_last, prompt_new, dec_new = pl.pallas_call(
        attend_kernel,
        name="attend",
        out_shape=(
            jax.ShapeDtypeStruct((ROWS, width), F32),
            jax.ShapeDtypeStruct((ROWS, 2 * DV), BF16),
            jax.ShapeDtypeStruct((width // 4, width), BF16),
            jax.ShapeDtypeStruct((PH, ROW_K, DV), F32),
            jax.ShapeDtypeStruct((4, HEADS, DK, DV), F32),
        ),
        in_specs=[hbm] * 12,
        out_specs=(vmem,) * 5,
        scratch_shapes=[
            pltpu.VMEM((OWN, PR, width), BF16),
            pltpu.VMEM((2, width), BF16),
            pltpu.VMEM((width, HEADS * DK), BF16),
            pltpu.VMEM((width, HEADS * DK), BF16),
            pltpu.VMEM((width, HEADS * DV), BF16),
            pltpu.VMEM((width, HEADS * DK), BF16),
            pltpu.VMEM((1, 2 * HEADS * DK), F32),
            pltpu.VMEM((1, width), F32),
            pltpu.VMEM((1, width), F32),
            pltpu.VMEM((PH, ROW_K, DV), F32),
            pltpu.VMEM((4, HEADS, DK, DV), F32),
            pltpu.VMEM((3, width // 4, width), BF16),
            pltpu.VMEM((RP, width), F32),
            pltpu.VMEM((2, ROWS, width), BF16),
            pltpu.VMEM((HEADS, 2, ROWS, DK), BF16),
            pltpu.VMEM((HEADS, 2, ROWS, DK), BF16),
            pltpu.VMEM((HEADS, 2, ROWS, DV), BF16),
            pltpu.VMEM((HEADS, 2, ROWS, DK), F32),
            pltpu.VMEM((HEADS, 2, PR, OWN, DK), F32),
            pltpu.VMEM((2, KVN, 4, ROW_K, DV), BF16),
            pltpu.VMEM((DK, DK), F32),
            pltpu.VMEM((KVN, ROW_K, DK), F32),
            pltpu.VMEM((2, KVN, 4, ROW_K, DV), BF16),
            pltpu.VMEM((KVN, ROW_K, DK), F32),
            pltpu.VMEM((2, KVN, 4, ROW_K, DV), BF16),
            pltpu.VMEM((2, KVN, 4, ROW_K, DV), BF16),
            pltpu.VMEM((PH, 2, OWN, DV), F32),
            pltpu.VMEM((PH, 2, OWN, DK), BF16),
            pltpu.VMEM((2, 2, ROWS, 2 * DV), BF16),
            pltpu.VMEM((ROWS, 2 * DV), BF16),
            dma((11,)),
            dma((4,)),
            dma((2,)),
            dma((2, KVN)),
            dma((2, KVN)),
            dma((KVN,)),
            dma((KVN,)),
            dma((2, KVN)),
            dma((2, KVN)),
            dma((4,)),
        ],
        compiler_params=pltpu.CompilerParams(collective_id=0, has_side_effects=True, vmem_limit_bytes=40 * 1024 * 1024),
    )(
        *(
            pltpu.with_memory_space_constraint(a, pltpu.HBM)
            for a in (
                pieces, new_tokens, w_query, w_key, w_value, w_decay, decay_bias.reshape(1, -1), norm_gain.reshape(1, -1),
                head_gain.reshape(1, -1), prompt_state.reshape(PH, ROW_K, DV), decode_state, w_out,
            )
        )
    )
    mixed, mixed_dec, prompt_out, dec_out = pl.pallas_call(
        finish_kernel,
        name="finish",
        out_shape=(
            jax.ShapeDtypeStruct((OWN, PR, width), BF16),
            jax.ShapeDtypeStruct((2, width), BF16),
            jax.ShapeDtypeStruct((PH, ROW_K, DV), F32),
            jax.ShapeDtypeStruct((4, HEADS, DK, DV), F32),
        ),
        in_specs=[vmem] * 5,
        out_specs=(hbm,) * 4,
        scratch_shapes=[
            pltpu.VMEM((OWN, PR, width), BF16),
            pltpu.VMEM((2, width), BF16),
            dma((3,)),
            dma((width // 256,)),
        ],
        compiler_params=pltpu.CompilerParams(vmem_limit_bytes=24 * 1024 * 1024),
    )(acc, peer, w_last, prompt_new, dec_new)
    return (
        mixed,
        mixed_dec,
        prompt_out.reshape(prompt_state.shape),
        dec_out,
    )


def solution(mesh):
    kv_tp, dp_kv_tp = ("kv", "tp"), ("dp", "kv", "tp")
    return jax.shard_map(
        on_device,
        mesh=mesh,
        in_specs=(
            P(kv_tp, "dp", None),
            P(dp_kv_tp, None),
            P(None, "tp"),
            P(None, "tp"),
            P(None, "tp"),
            P(None, "tp"),
            P(),
            P(),
            P(),
            P(),
            P("dp", "tp", "kv", None),
            P(("dp", "kv"), "tp", None, None),
        ),
        out_specs=(
            P(kv_tp, "dp", None),
            P(dp_kv_tp, None),
            P("dp", "tp", "kv", None),
            P(("dp", "kv"), "tp", None, None),
        ),
        check_vma=False,
    )
```

time: 45.3 us -> 45.3 us (level)
    pallas_call x1, Pallas kernels: 39.4 us -> 41.6 us  [on_device(): pl.pallas_call(attend_kernel, name='attend', out_shape=(jax.ShapeDtypeStr...]
    pallas_call x1, Pallas kernels: 5.14 us -> 2.98 us  [on_device(): pl.pallas_call(finish_kernel, name='finish', out_shape=(jax.ShapeDtypeStr...]
where the time goes in v3:
time: 45.3 us; the launch traced here: 45.2 us
  Pallas kernels  44.6 us (98%)
  between operations  0.64 us (1%)
    pallas_call x1, Pallas kernels, on_device(): pl.pallas_call(attend_kernel, name='attend', out_shape=(jax.ShapeDtypeStr...  41.6 us
    pallas_call x1, Pallas kernels, on_device(): pl.pallas_call(finish_kernel, name='finish', out_shape=(jax.ShapeDtypeStr...  2.98 us

profile of v3, /device:TPU:1, one launch (start us, length us, event | category | flops | bytes accessed | tf_op | source)
XLA Modules:
  0.0 45.2 jit_solution(11041052705137707543)
XLA Ops:
  0.6 41.6 %attend.1 = (f32[272,2048]{1,0:T(8,128)S(1)}, bf16[272,512]{1,0:T(8,128)(2,1)S(1)}, bf16[512,2048]{1,0:T(8,128)(2,1)S(1)}, f32[8,8,256]{2,1,0:T(8,128)S(1)}, f32[4,4,128,256]{3,2,1,0:T(8,128)S(1)}) custom-call(bf16[128,2,2048]{2,1,0:T(2,128)(2,1)} %pieces.1, bf16[2,2048]{1,0:T(2,128)(2,1)} %new_tokens.1, bf16[2048,512]{1,0:T(8,128)(2,1)} %w_query.1, ...), custom_call_target="tpu_custom_call" | custom-call | tf_op jit(solution)/shard_map/attend/pallas_call | solution.py:425
  42.2 3.0 %finish.1 = (bf16[128,2,2048]{2,1,0:T(2,128)(2,1)}, bf16[2,2048]{1,0:T(2,128)(2,1)}, f32[8,8,256]{2,1,0:T(8,128)}, f32[4,4,128,256]{3,2,1,0:T(8,128)}) custom-call(f32[272,2048]{1,0:T(8,128)S(1)} %get-tuple-element.13.acc, bf16[272,512]{1,0:T(8,128)(2,1)S(1)} %get-tuple-element.14.peer, bf16[512,2048]{1,0:T(8,128)(2,1)S(1)} %get-tuple-element.15.w_last, ...), custom_call_target="tpu_custom_call" | custom-call | tf_op jit(solution)/shard_map/finish/pallas_call | solution.py:489

commit v4 on v3

--- a/solution.py
+++ b/solution.py
@@ -59,7 +59,7 @@
     pieces, new_tokens, w_query, w_key, w_value, w_decay, bias, gain, head_gain, prompt_state, decode_state, w_out,
     acc, peer, w_last, prompt_out, dec_new,
     x3, nt, wq, wk, wv, wd, bias_v, gain_v, hg_v, ps, ds, wo, xs, rows, qb, kb, vb, db, bb, st, tt, ttt, rs, rt, sb, inc,
-    att, sqc, nrm, peer0, load_sem, wo_sem, row_sem, st_send, st_recv, tt_send, tt_recv, in_send, in_recv, nrm_sem,
+    att, sqc, nrm, load_sem, wo_sem, row_sem, st_send, st_recv, tt_send, tt_recv, in_send, in_recv, nrm_sem,
 ):
     kv = lax.axis_index("kv")
     tp = lax.axis_index("tp")
@@ -215,13 +215,13 @@
             state_copy(s, to, kv).start()
         rs[s, kv] = st[s, kv]
 
-    quarter = width // 4
-
-    def out_rows(i):
-        owner = tp if i < 2 else other
-        return w_out.at[pl.ds(pl.multiple_of((2 * owner + i % 2) * quarter, quarter), quarter)]
-
-    out_loads = [pltpu.make_async_copy(out_rows(i), wo.at[i] if i < 3 else w_last, wo_sem.at[i]) for i in range(4)]
+    def out_rows(owner):
+        return w_out.at[pl.ds(pl.multiple_of(owner * (width // 2), width // 2), width // 2)]
+
+    out_loads = [
+        pltpu.make_async_copy(out_rows(tp), wo, wo_sem.at[0]),
+        pltpu.make_async_copy(out_rows(other), w_last, wo_sem.at[1]),
+    ]
     for copy in out_loads:
         copy.start()
     load_q.wait()
@@ -282,9 +282,33 @@
         sqc[i, 1] = (qs[1] * jnp.exp(bs[1] + t0)).astype(BF16)
         return 0
 
-    lax.fori_loop(0, PH, inside, 0)
-
-    for copy in (load_ps, load_ds, load_hg):
+    lax.fori_loop(0, PH // 2, inside, 0)
+
+    def scan(s):
+        for frm in peers:
+            if s == 0:
+                total_copy(frm, frm).wait_recv()
+            state_copy(s, frm, frm).wait_recv()
+        at = [(m // 2) * HEADS + 2 * s + m % 2 for m in range(4)]
+        state = [ps[n] for n in at]
+        for i in range(KVN):
+            decay = jnp.exp(rt[i])
+            for m in range(4):
+                sb[s, i, m] = state[m].astype(BF16)
+                n = s * 4 + m
+                state[m] = decay[:, n : n + 1] * state[m] + rs[s, i, m].astype(F32)
+        for to in peers:
+            back_copy(s, to, kv).start()
+        inc[s, kv] = sb[s, kv]
+        for n, last in zip(at, state):
+            prompt_out[n] = last
+
+    load_ps.wait()
+    scan(0)
+    scan(1)
+    lax.fori_loop(PH // 2, PH, inside, 0)
+
+    for copy in (load_ds, load_hg):
         copy.wait()
 
     def normed(out, h):
@@ -319,45 +343,11 @@
                 n = token * HEADS + h
                 dec_new[token, h] = columns[:, n : n + 1] * ds[token, h] + fresh
 
-    for to in peers:
-        total_copy(to, to).wait_recv()
-    for s in range(2):
-        for frm in peers:
-            state_copy(s, frm, frm).wait_recv()
-
-        def scan_step(i, state):
-            decay = jnp.exp(rt[i])
-            after = []
-            for m in range(4):
-                sb[s, i, m] = state[m].astype(BF16)
-                after.append(decay[:, s * 4 + m : s * 4 + m + 1] * state[m] + rs[s, i, m].astype(F32))
-            return tuple(after)
-
-        at = [(m // 2) * HEADS + 2 * s + m % 2 for m in range(4)]
-        last = lax.fori_loop(0, KVN, scan_step, tuple(ps[n] for n in at))
-        for to in peers:
-            back_copy(s, to, kv).start()
-        inc[s, kv] = sb[s, kv]
-        for n, state in zip(at, last):
-            prompt_out[n] = state
-
     def nrm_copy(s):
         return pltpu.make_async_remote_copy(
-            src_ref=nrm.at[other, s], dst_ref=peer0 if s == 0 else peer, send_sem=nrm_sem.at[s], recv_sem=nrm_sem.at[2 + s],
+            src_ref=nrm.at[other, s], dst_ref=peer.at[s], send_sem=nrm_sem.at[s], recv_sem=nrm_sem.at[2 + s],
             device_id={"tp": other}, device_id_type=MESH,
         )
-
-    def add_product(lhs, weights, fresh):
-        left = jnp.concatenate([dotg(order, lhs[:RP], TN).astype(BF16), lhs[RP:]], axis=0)
-        tile = 256
-
-        def body(n, _):
-            cols = pl.ds(pl.multiple_of(n * tile, tile), tile)
-            got = dot(left, weights[:, cols])
-            acc[:, cols] = got if fresh else acc[:, cols] + got
-            return 0
-
-        lax.fori_loop(0, width // tile, body, 0)
 
     for s in range(2):
         for frm in peers:
@@ -370,18 +360,31 @@
                     out = att[4 * s + m, half] + dot(sqc[4 * s + m, half], incoming)
                     nrm[half, s, p * OWN : (p + 1) * OWN, e * DV : (e + 1) * DV] = normed(out, 2 * s + e)
         nrm_copy(s).start()
-        out_loads[s].wait()
-        add_product(nrm[tp, s], wo.at[s], s == 0)
+
+    for copy in out_loads:
+        copy.wait()
+    left = in_position_order(order, nrm, tp)
+    tile = 256
+
+    def own_product(n, _):
+        cols = pl.ds(pl.multiple_of(n * tile, tile), tile)
+        acc[:, cols] = dot(left, wo[:, cols])
+        return 0
+
+    lax.fori_loop(0, width // tile, own_product, 0)
+    for s in range(2):
         nrm_copy(s).wait()
-        if s == 0:
-            out_loads[2].wait()
-            add_product(peer0[...], wo.at[2], False)
-    out_loads[3].wait()
     for to in peers:
         total_copy(to, kv).wait_send()
         for s in range(2):
             state_copy(s, to, kv).wait_send()
             back_copy(s, to, kv).wait_send()
+
+
+def in_position_order(order, rows_ref, half):
+    cut = [rows_ref[half, s] if half is not None else rows_ref[s] for s in range(2)]
+    parts = [jnp.concatenate([dotg(order, part[:RP], TN).astype(BF16), part[RP:]], axis=0) for part in cut]
+    return jnp.concatenate(parts, axis=1)
 
 
 def finish_kernel(acc, peer, w_last, prompt_in, dec_in, mixed, mixed_dec, prompt_out, dec_out, out3, out2, sem, tile_sem):
@@ -390,7 +393,7 @@
     for copy in copies:
         copy.start()
     order = order_matrix()
-    left = jnp.concatenate([dotg(order, peer[:RP], TN).astype(BF16), peer[RP:]], axis=0)
+    left = in_position_order(order, peer, None)
     tile = 256
 
     def out_copy(n):
@@ -427,8 +430,8 @@
         name="attend",
         out_shape=(
             jax.ShapeDtypeStruct((ROWS, width), F32),
-            jax.ShapeDtypeStruct((ROWS, 2 * DV), BF16),
-            jax.ShapeDtypeStruct((width // 4, width), BF16),
+            jax.ShapeDtypeStruct((2, ROWS, 2 * DV), BF16),
+            jax.ShapeDtypeStruct((width // 2, width), BF16),
             jax.ShapeDtypeStruct((PH, ROW_K, DV), F32),
             jax.ShapeDtypeStruct((4, HEADS, DK, DV), F32),
         ),
@@ -446,7 +449,7 @@
             pltpu.VMEM((1, width), F32),
             pltpu.VMEM((PH, ROW_K, DV), F32),
             pltpu.VMEM((4, HEADS, DK, DV), F32),
-            pltpu.VMEM((3, width // 4, width), BF16),
+            pltpu.VMEM((width // 2, width), BF16),
             pltpu.VMEM((RP, width), F32),
             pltpu.VMEM((2, ROWS, width), BF16),
             pltpu.VMEM((HEADS, 2, ROWS, DK), BF16),
@@ -464,9 +467,8 @@
             pltpu.VMEM((PH, 2, OWN, DV), F32),
             pltpu.VMEM((PH, 2, OWN, DK), BF16),
             pltpu.VMEM((2, 2, ROWS, 2 * DV), BF16),
-            pltpu.VMEM((ROWS, 2 * DV), BF16),
             dma((11,)),
-            dma((4,)),
+            dma((2,)),
             dma((2,)),
             dma((2, KVN)),
             dma((2, KVN)),

time: 45.3 us -> 38.7 us (0.85); the launches traced: 45.2 us -> 38.1 us
  Pallas kernels: 44.6 us -> 37.4 us
    pallas_call x1, Pallas kernels: 41.6 us -> 33.7 us  [on_device(): pl.pallas_call(attend_kernel, name='attend', out_shape=(jax.ShapeDtypeStr...]
    pallas_call x1, Pallas kernels: 2.98 us -> 3.72 us  [on_device(): pl.pallas_call(finish_kernel, name='finish', out_shape=(jax.ShapeDtypeStr...]
where the time goes in v4:
time: 38.7 us; the launch traced here: 38.1 us
  Pallas kernels  37.4 us (97%)
  between operations  0.64 us (2%)
    pallas_call x1, Pallas kernels, on_device(): pl.pallas_call(attend_kernel, name='attend', out_shape=(jax.ShapeDtypeStr...  33.7 us
    pallas_call x1, Pallas kernels, on_device(): pl.pallas_call(finish_kernel, name='finish', out_shape=(jax.ShapeDtypeStr...  3.72 us

profile of v4, /device:TPU:1, one launch (start us, length us, event | category | flops | bytes accessed | tf_op | source)
XLA Modules:
  0.0 38.1 jit_solution(7829056786355527593)
XLA Ops:
  0.6 33.7 %attend.1 = (f32[272,2048]{1,0:T(8,128)S(1)}, bf16[2,272,512]{2,1,0:T(8,128)(2,1)S(1)}, bf16[1024,2048]{1,0:T(8,128)(2,1)S(1)}, f32[8,8,256]{2,1,0:T(8,128)S(1)}, f32[4,4,128,256]{3,2,1,0:T(8,128)S(1)}) custom-call(bf16[128,2,2048]{2,1,0:T(2,128)(2,1)} %pieces.1, bf16[2,2048]{1,0:T(2,128)(2,1)} %new_tokens.1, bf16[2048,512]{1,0:T(8,128)(2,1)} %w_query.1, ...), custom_call_target="tpu_custom_call" | custom-call | tf_op jit(solution)/shard_map/attend/pallas_call | solution.py:428
  34.4 3.7 %finish.1 = (bf16[128,2,2048]{2,1,0:T(2,128)(2,1)}, bf16[2,2048]{1,0:T(2,128)(2,1)}, f32[8,8,256]{2,1,0:T(8,128)}, f32[4,4,128,256]{3,2,1,0:T(8,128)}) custom-call(f32[272,2048]{1,0:T(8,128)S(1)} %get-tuple-element.13.acc, bf16[2,272,512]{2,1,0:T(8,128)(2,1)S(1)} %get-tuple-element.14.peer, bf16[1024,2048]{1,0:T(8,128)(2,1)S(1)} %get-tuple-element.15.w_last, ...), custom_call_target="tpu_custom_call" | custom-call | tf_op jit(solution)/shard_map/finish/pallas_call | solution.py:491

commit v5 on v4

--- a/solution.py
+++ b/solution.py
@@ -59,7 +59,7 @@
     pieces, new_tokens, w_query, w_key, w_value, w_decay, bias, gain, head_gain, prompt_state, decode_state, w_out,
     acc, peer, w_last, prompt_out, dec_new,
     x3, nt, wq, wk, wv, wd, bias_v, gain_v, hg_v, ps, ds, wo, xs, rows, qb, kb, vb, db, bb, st, tt, ttt, rs, rt, sb, inc,
-    att, sqc, nrm, load_sem, wo_sem, row_sem, st_send, st_recv, tt_send, tt_recv, in_send, in_recv, nrm_sem,
+    att, sqc, nrm, peer0, load_sem, wo_sem, row_sem, st_send, st_recv, tt_send, tt_recv, in_send, in_recv, nrm_sem,
 ):
     kv = lax.axis_index("kv")
     tp = lax.axis_index("tp")
@@ -93,7 +93,7 @@
     order = order_matrix()
     for copy in (load_x, load_nt, load_gain):
         copy.wait()
-    for copy in (load_k, load_v):
+    for copy in (load_k, load_v, load_q):
         copy.start()
     flat = x3[...].reshape(RP, width)
     step = 512
@@ -111,45 +111,43 @@
     nt_rows = wide * nt_factor * gain_v[...]
     rows[tp, RP:, :] = jnp.concatenate([nt_rows, jnp.zeros((PAD - nt_rows.shape[0], width), F32)], axis=0).astype(BF16)
 
+    def project(half, weights, out, kind, first, count):
+        per = 2 * DK
+
+        for j in range(first, first + count):
+            got = dot(rows[half], weights[:, j * per : (j + 1) * per])
+            if kind == "v":
+                out[j, half] = got.astype(BF16)
+                continue
+            for e in range(2):
+                part = got[:, e * DK : (e + 1) * DK]
+                if kind == "q":
+                    part = (part * DK**-0.5).astype(BF16)
+                elif kind == "k":
+                    part = part.astype(BF16)
+                else:
+                    at = pl.multiple_of(tp * (HEADS * DK) + j * per + e * DK, DK)
+                    part = log_decay(part + bias_v[:, pl.ds(at, DK)])
+                out[2 * j + e, half] = part
+
+    load_bias.wait()
+    load_d.wait()
+    project(tp, wd, db, "d", 0, 2)
     pl.semaphore_wait(barrier, KVN)
     row_copy = pltpu.make_async_remote_copy(
         src_ref=rows.at[tp], dst_ref=rows.at[tp], send_sem=row_sem.at[0], recv_sem=row_sem.at[1],
         device_id={"tp": other}, device_id_type=MESH,
     )
     row_copy.start()
-    for copy in (load_q, load_ds, load_ps, load_hg):
+    for copy in (load_ds, load_ps, load_hg):
         copy.start()
 
-    def project(half, weights, out, kind, first, count):
-        per = 2 * DK
-
-        def tile(j, _):
-            cols = pl.ds(pl.multiple_of(j * per, per), per)
-            got = dot(rows[half], weights[:, cols])
-            if kind == "v":
-                out[j, half] = got.astype(BF16)
-            else:
-                for e in range(2):
-                    part = got[:, e * DK : (e + 1) * DK]
-                    if kind == "q":
-                        part = (part * DK**-0.5).astype(BF16)
-                    elif kind == "k":
-                        part = part.astype(BF16)
-                    else:
-                        at = pl.multiple_of(tp * (HEADS * DK) + j * per + e * DK, DK)
-                        part = log_decay(part + bias_v[:, pl.ds(at, DK)])
-                    out[2 * j + e, half] = part
-            return 0
-
-        lax.fori_loop(first, first + count, tile, 0)
-
-    load_bias.wait()
-    load_d.wait()
-    project(tp, wd, db, "d", 0, 2)
     load_k.wait()
     project(tp, wk, kb, "k", 0, 2)
     load_v.wait()
     project(tp, wv, vb, "v", 0, 4)
+    load_q.wait()
+    project(tp, wq, qb, "q", 0, 2)
     row_copy.wait()
     project(other, wd, db, "d", 0, 2)
 
@@ -215,26 +213,26 @@
             state_copy(s, to, kv).start()
         rs[s, kv] = st[s, kv]
 
-    def out_rows(owner):
-        return w_out.at[pl.ds(pl.multiple_of(owner * (width // 2), width // 2), width // 2)]
-
-    out_loads = [
-        pltpu.make_async_copy(out_rows(tp), wo, wo_sem.at[0]),
-        pltpu.make_async_copy(out_rows(other), w_last, wo_sem.at[1]),
-    ]
+    quarter = width // 4
+
+    def out_load(i):
+        owner = tp if i < 2 else other
+        src = w_out.at[pl.ds(pl.multiple_of((2 * owner + i % 2) * quarter, quarter), quarter)]
+        dst = wo.at[i * quarter : (i + 1) * quarter] if i < 3 else w_last
+        return pltpu.make_async_copy(src, dst, wo_sem.at[i])
+
+    out_loads = [out_load(i) for i in range(4)]
     for copy in out_loads:
         copy.start()
-    load_q.wait()
-    project(0, wq, qb, "q", 0, 2)
-    project(1, wq, qb, "q", 0, 2)
+    project(other, wq, qb, "q", 0, 2)
 
     t_in = lax.broadcasted_iota(jnp.int32, (BLK, BLK), 0)
     s_in = lax.broadcasted_iota(jnp.int32, (BLK, BLK), 1)
     keep = t_in >= s_in
 
-    def inside(i, _):
+    def inside(i):
         p, h = (i // 2) % 2, 2 * (i // 4) + i % 2
-        at = pl.ds(pl.multiple_of(p * OWN, OWN), OWN)
+        at = slice(p * OWN, (p + 1) * OWN)
         ks = [kb[h, half, at].astype(F32) for half in range(2)]
         qs = [qb[h, half, at].astype(F32) for half in range(2)]
         bs = [bb[h, half, p] for half in range(2)]
@@ -280,9 +278,9 @@
             att[i, half, lo : lo + BLK] = out
         sqc[i, 0] = (qs[0] * jnp.exp(bs[0])).astype(BF16)
         sqc[i, 1] = (qs[1] * jnp.exp(bs[1] + t0)).astype(BF16)
-        return 0
-
-    lax.fori_loop(0, PH // 2, inside, 0)
+
+    for i in range(PH // 2):
+        inside(i)
 
     def scan(s):
         for frm in peers:
@@ -305,8 +303,9 @@
 
     load_ps.wait()
     scan(0)
+    for i in range(PH // 2, PH):
+        inside(i)
     scan(1)
-    lax.fori_loop(PH // 2, PH, inside, 0)
 
     for copy in (load_ds, load_hg):
         copy.wait()
@@ -345,10 +344,11 @@
 
     def nrm_copy(s):
         return pltpu.make_async_remote_copy(
-            src_ref=nrm.at[other, s], dst_ref=peer.at[s], send_sem=nrm_sem.at[s], recv_sem=nrm_sem.at[2 + s],
+            src_ref=nrm.at[other, s], dst_ref=peer0 if s == 0 else peer, send_sem=nrm_sem.at[s], recv_sem=nrm_sem.at[2 + s],
             device_id={"tp": other}, device_id_type=MESH,
         )
 
+    tile = 256
     for s in range(2):
         for frm in peers:
             back_copy(s, frm, frm).wait_recv()
@@ -360,20 +360,21 @@
                     out = att[4 * s + m, half] + dot(sqc[4 * s + m, half], incoming)
                     nrm[half, s, p * OWN : (p + 1) * OWN, e * DV : (e + 1) * DV] = normed(out, 2 * s + e)
         nrm_copy(s).start()
-
-    for copy in out_loads:
-        copy.wait()
-    left = in_position_order(order, nrm, tp)
-    tile = 256
-
-    def own_product(n, _):
-        cols = pl.ds(pl.multiple_of(n * tile, tile), tile)
-        acc[:, cols] = dot(left, wo[:, cols])
-        return 0
-
-    lax.fori_loop(0, width // tile, own_product, 0)
-    for s in range(2):
-        nrm_copy(s).wait()
+        left = in_position_order(order, nrm[tp, s])
+        out_loads[s].wait()
+        if s == 0:
+            for n in range(width // tile):
+                cols = slice(n * tile, (n + 1) * tile)
+                acc[:, cols] = dot(left, wo[:quarter, cols])
+        else:
+            out_loads[2].wait()
+            nrm_copy(0).wait()
+            left = jnp.concatenate([left, in_position_order(order, peer0[...])], axis=1)
+            for n in range(width // tile):
+                cols = slice(n * tile, (n + 1) * tile)
+                acc[:, cols] += dot(left, wo[quarter:, cols])
+    nrm_copy(1).wait()
+    out_loads[3].wait()
     for to in peers:
         total_copy(to, kv).wait_send()
         for s in range(2):
@@ -381,10 +382,8 @@
             back_copy(s, to, kv).wait_send()
 
 
-def in_position_order(order, rows_ref, half):
-    cut = [rows_ref[half, s] if half is not None else rows_ref[s] for s in range(2)]
-    parts = [jnp.concatenate([dotg(order, part[:RP], TN).astype(BF16), part[RP:]], axis=0) for part in cut]
-    return jnp.concatenate(parts, axis=1)
+def in_position_order(order, part):
+    return jnp.concatenate([dotg(order, part[:RP], TN).astype(BF16), part[RP:]], axis=0)
 
 
 def finish_kernel(acc, peer, w_last, prompt_in, dec_in, mixed, mixed_dec, prompt_out, dec_out, out3, out2, sem, tile_sem):
@@ -393,22 +392,20 @@
     for copy in copies:
         copy.start()
     order = order_matrix()
-    left = in_position_order(order, peer, None)
+    left = in_position_order(order, peer[...])
     tile = 256
 
     def out_copy(n):
-        cols = pl.ds(pl.multiple_of(n * tile, tile), tile)
+        cols = slice(n * tile, (n + 1) * tile)
         return pltpu.make_async_copy(out3.at[:, :, cols], mixed.at[:, :, cols], tile_sem.at[n])
 
-    def body(n, _):
-        cols = pl.ds(pl.multiple_of(n * tile, tile), tile)
+    for n in range(width // tile):
+        cols = slice(n * tile, (n + 1) * tile)
         got = (acc[:, cols] + dot(left, w_last[:, cols])).astype(BF16)
         out3[:, :, cols] = got[:RP].reshape(OWN, PR, tile)
         out2[:, cols] = got[RP : RP + 2]
         out_copy(n).start()
-        return 0
-
-    lax.fori_loop(0, width // tile, body, 0)
+
     last = pltpu.make_async_copy(out2, mixed_dec, sem.at[2])
     last.start()
     for n in range(width // tile):
@@ -430,8 +427,8 @@
         name="attend",
         out_shape=(
             jax.ShapeDtypeStruct((ROWS, width), F32),
-            jax.ShapeDtypeStruct((2, ROWS, 2 * DV), BF16),
-            jax.ShapeDtypeStruct((width // 2, width), BF16),
+            jax.ShapeDtypeStruct((ROWS, 2 * DV), BF16),
+            jax.ShapeDtypeStruct((width // 4, width), BF16),
             jax.ShapeDtypeStruct((PH, ROW_K, DV), F32),
             jax.ShapeDtypeStruct((4, HEADS, DK, DV), F32),
         ),
@@ -449,7 +446,7 @@
             pltpu.VMEM((1, width), F32),
             pltpu.VMEM((PH, ROW_K, DV), F32),
             pltpu.VMEM((4, HEADS, DK, DV), F32),
-            pltpu.VMEM((width // 2, width), BF16),
+            pltpu.VMEM((3 * width // 4, width), BF16),
             pltpu.VMEM((RP, width), F32),
             pltpu.VMEM((2, ROWS, width), BF16),
             pltpu.VMEM((HEADS, 2, ROWS, DK), BF16),
@@ -467,8 +464,9 @@
             pltpu.VMEM((PH, 2, OWN, DV), F32),
             pltpu.VMEM((PH, 2, OWN, DK), BF16),
             pltpu.VMEM((2, 2, ROWS, 2 * DV), BF16),
+            pltpu.VMEM((ROWS, 2 * DV), BF16),
             dma((11,)),
-            dma((2,)),
+            dma((4,)),
             dma((2,)),
             dma((2, KVN)),
             dma((2, KVN)),

time: 38.7 us -> 35.7 us (0.922); the launches traced: 38.1 us -> 35.6 us
  Pallas kernels: 37.4 us -> 34.8 us
    pallas_call x1, Pallas kernels: 33.7 us -> 32.4 us  [on_device(): pl.pallas_call(attend_kernel, name='attend', out_shape=(jax.ShapeDtypeStr...]
    pallas_call x1, Pallas kernels: 3.72 us -> 2.4 us  [on_device(): pl.pallas_call(finish_kernel, name='finish', out_shape=(jax.ShapeDtypeStr...]
where the time goes in v5:
time: 35.7 us; the launch traced here: 35.6 us
  Pallas kernels  34.8 us (97%)
  between operations  0.8 us (2%)
    pallas_call x1, Pallas kernels, on_device(): pl.pallas_call(attend_kernel, name='attend', out_shape=(jax.ShapeDtypeStr...  32.4 us
    pallas_call x1, Pallas kernels, on_device(): pl.pallas_call(finish_kernel, name='finish', out_shape=(jax.ShapeDtypeStr...  2.4 us

profile of v5, /device:TPU:1, one launch (start us, length us, event | category | flops | bytes accessed | tf_op | source)
XLA Modules:
  0.0 35.6 jit_solution(1287866316615170730)
XLA Ops:
  0.6 32.4 %attend.1 = (f32[272,2048]{1,0:T(8,128)S(1)}, bf16[272,512]{1,0:T(8,128)(2,1)S(1)}, bf16[512,2048]{1,0:T(8,128)(2,1)S(1)}, f32[8,8,256]{2,1,0:T(8,128)S(1)}, f32[4,4,128,256]{3,2,1,0:T(8,128)S(1)}) custom-call(bf16[128,2,2048]{2,1,0:T(2,128)(2,1)} %pieces.1, bf16[2,2048]{1,0:T(2,128)(2,1)} %new_tokens.1, bf16[2048,512]{1,0:T(8,128)(2,1)} %w_query.1, ...), custom_call_target="tpu_custom_call" | custom-call | tf_op jit(solution)/shard_map/attend/pallas_call | solution.py:425
  33.0 2.4 %finish.1 = (bf16[128,2,2048]{2,1,0:T(2,128)(2,1)}, bf16[2,2048]{1,0:T(2,128)(2,1)}, f32[8,8,256]{2,1,0:T(8,128)}, f32[4,4,128,256]{3,2,1,0:T(8,128)}) custom-call(f32[272,2048]{1,0:T(8,128)S(1)} %get-tuple-element.13.acc, bf16[272,512]{1,0:T(8,128)(2,1)S(1)} %get-tuple-element.14.peer, bf16[512,2048]{1,0:T(8,128)(2,1)S(1)} %get-tuple-element.15.w_last, ...), custom_call_target="tpu_custom_call" | custom-call | tf_op jit(solution)/shard_map/finish/pallas_call | solution.py:489

commit v6 on v5

--- a/solution.py
+++ b/solution.py
@@ -27,6 +27,7 @@
 SIDE = 4
 ROW_K = DK // KVN
 PH = PR * HEADS
+STAGES = ((0,), (1, 2), (3,))
 TN = (((0,), (0,)), ((), ()))
 NT = (((1,), (1,)), ((), ()))
 
@@ -58,13 +59,15 @@
 def attend_kernel(
     pieces, new_tokens, w_query, w_key, w_value, w_decay, bias, gain, head_gain, prompt_state, decode_state, w_out,
     acc, peer, w_last, prompt_out, dec_new,
-    x3, nt, wq, wk, wv, wd, bias_v, gain_v, hg_v, ps, ds, wo, xs, rows, qb, kb, vb, db, bb, st, tt, ttt, rs, rt, sb, inc,
-    att, sqc, nrm, peer0, load_sem, wo_sem, row_sem, st_send, st_recv, tt_send, tt_recv, in_send, in_recv, nrm_sem,
+    x3, nt, wq, wk, wv, wd, bias_v, gain_v, hg_v, ps, ds, wo, xs, rows, qb, kb, vb, db, bb, tt, ttt, rt,
+    st0, st1, st2, rs0, rs1, rs2, sb0, sb1, sb2, inc0, inc1, inc2, peer0, peer1,
+    att, sqc, nrm, load_sem, wo_sem, row_sem, st_sem, tt_sem, in_sem, nrm_sem,
 ):
     kv = lax.axis_index("kv")
     tp = lax.axis_index("tp")
     other = 1 - tp
     width = rows.shape[-1]
+    st, rs, sb, inc = (st0, st1, st2), (rs0, rs1, rs2), (sb0, sb1, sb2), (inc0, inc1, inc2)
 
     def load(i, src, dst):
         return pltpu.make_async_copy(src, dst, load_sem.at[i])
@@ -146,8 +149,6 @@
     project(tp, wk, kb, "k", 0, 2)
     load_v.wait()
     project(tp, wv, vb, "v", 0, 4)
-    load_q.wait()
-    project(tp, wq, qb, "q", 0, 2)
     row_copy.wait()
     project(other, wd, db, "d", 0, 2)
 
@@ -168,39 +169,44 @@
             for h in range(HEADS):
                 bb[h, half, p] = got[:, h * DK : (h + 1) * DK]
         for h in range(HEADS):
-            n = (h // 2) * 4 + p * 2 + h % 2
+            n = h * PR + p
             tt[n : n + 1, :] = total[:, h * DK : (h + 1) * DK]
     ttt[...] = tt[...].T.reshape(KVN, ROW_K, DK)
 
     def total_copy(to, slot):
         return pltpu.make_async_remote_copy(
-            src_ref=ttt.at[to], dst_ref=rt.at[slot], send_sem=tt_send.at[to], recv_sem=tt_recv.at[slot],
+            src_ref=ttt.at[to], dst_ref=rt.at[slot], send_sem=tt_sem.at[0], recv_sem=tt_sem.at[1],
             device_id={"kv": to}, device_id_type=MESH,
         )
 
     def state_copy(s, to, slot):
         return pltpu.make_async_remote_copy(
-            src_ref=st.at[s, to], dst_ref=rs.at[s, slot], send_sem=st_send.at[s, to], recv_sem=st_recv.at[s, slot],
+            src_ref=st[s].at[to], dst_ref=rs[s].at[slot], send_sem=st_sem.at[0, s], recv_sem=st_sem.at[1, s],
             device_id={"kv": to}, device_id_type=MESH,
         )
 
     def back_copy(s, to, slot):
         return pltpu.make_async_remote_copy(
-            src_ref=sb.at[s, to], dst_ref=inc.at[s, slot], send_sem=in_send.at[s, to], recv_sem=in_recv.at[s, slot],
+            src_ref=sb[s].at[to], dst_ref=inc[s].at[slot], send_sem=in_sem.at[0, s], recv_sem=in_sem.at[1, s],
             device_id={"kv": to}, device_id_type=MESH,
         )
+
+    def wait_all(ref, sem):
+        part = ref.at[: KVN - 1]
+        pltpu.make_async_copy(part, part, sem).wait()
 
     for to in peers:
         total_copy(to, kv).start()
     rt[kv] = ttt[kv]
 
-    for s in range(2):
-        project(other, wk, kb, "k", s, 1)
-        project(other, wv, vb, "v", 2 * s, 2)
-        for p in range(PR):
-            at = slice(p * OWN, (p + 1) * OWN)
-            for e in range(2):
-                h = 2 * s + e
+    for s, heads in enumerate(STAGES):
+        for h in heads:
+            if h in (0, 2):
+                project(other, wk, kb, "k", h // 2, 1)
+            project(other, wv, vb, "v", h, 1)
+        for e, h in enumerate(heads):
+            for p in range(PR):
+                at = slice(p * OWN, (p + 1) * OWN)
                 b0, b1 = bb[h, 0, p], bb[h, 1, p]
                 t0, t1 = b0[OWN - 1 :], b1[OWN - 1 :]
                 e0 = kb[h, 0, at].astype(F32) * jnp.exp((t0 - b0) + t1)
@@ -208,22 +214,24 @@
                 keys = jnp.concatenate([e0.astype(BF16), e1.astype(BF16)], axis=0)
                 vals = jnp.concatenate([vb[h, 0, at], vb[h, 1, at]], axis=0)
                 state = dotg(keys, vals, TN)
-                st[s, :, p * 2 + e] = state.reshape(KVN, ROW_K, DV).astype(BF16)
+                st[s][:, e * PR + p] = state.reshape(KVN, ROW_K, DV).astype(BF16)
         for to in peers:
             state_copy(s, to, kv).start()
-        rs[s, kv] = st[s, kv]
+        rs[s][kv] = st[s][kv]
 
     quarter = width // 4
 
     def out_load(i):
-        owner = tp if i < 2 else other
-        src = w_out.at[pl.ds(pl.multiple_of((2 * owner + i % 2) * quarter, quarter), quarter)]
-        dst = wo.at[i * quarter : (i + 1) * quarter] if i < 3 else w_last
+        owner, first, count = ((tp, 0, 4), (other, 0, 3), (other, 3, 1))[i]
+        src = w_out.at[pl.ds(pl.multiple_of(owner * (2 * quarter) + first * DV, DV), count * DV)]
+        dst = w_last if i == 2 else wo.at[pl.ds(4 * DV * i, count * DV)]
         return pltpu.make_async_copy(src, dst, wo_sem.at[i])
 
-    out_loads = [out_load(i) for i in range(4)]
+    out_loads = [out_load(i) for i in range(3)]
     for copy in out_loads:
         copy.start()
+    load_q.wait()
+    project(tp, wq, qb, "q", 0, 2)
     project(other, wq, qb, "q", 0, 2)
 
     t_in = lax.broadcasted_iota(jnp.int32, (BLK, BLK), 0)
@@ -231,7 +239,7 @@
     keep = t_in >= s_in
 
     def inside(i):
-        p, h = (i // 2) % 2, 2 * (i // 4) + i % 2
+        p, h = i % PR, i // PR
         at = slice(p * OWN, (p + 1) * OWN)
         ks = [kb[h, half, at].astype(F32) for half in range(2)]
         qs = [qb[h, half, at].astype(F32) for half in range(2)]
@@ -283,22 +291,20 @@
         inside(i)
 
     def scan(s):
-        for frm in peers:
-            if s == 0:
-                total_copy(frm, frm).wait_recv()
-            state_copy(s, frm, frm).wait_recv()
-        at = [(m // 2) * HEADS + 2 * s + m % 2 for m in range(4)]
-        state = [ps[n] for n in at]
+        if s == 0:
+            wait_all(rt, tt_sem.at[1])
+        wait_all(rs[s], st_sem.at[1, s])
+        chains = [(e * PR + p, p * HEADS + h, h * PR + p) for e, h in enumerate(STAGES[s]) for p in range(PR)]
+        state = [ps[n] for _, n, _ in chains]
         for i in range(KVN):
             decay = jnp.exp(rt[i])
-            for m in range(4):
-                sb[s, i, m] = state[m].astype(BF16)
-                n = s * 4 + m
-                state[m] = decay[:, n : n + 1] * state[m] + rs[s, i, m].astype(F32)
+            for j, (m, _, lane) in enumerate(chains):
+                sb[s][i, m] = state[j].astype(BF16)
+                state[j] = decay[:, lane : lane + 1] * state[j] + rs[s][i, m].astype(F32)
         for to in peers:
             back_copy(s, to, kv).start()
-        inc[s, kv] = sb[s, kv]
-        for n, last in zip(at, state):
+        inc[s][kv] = sb[s][kv]
+        for (_, n, _), last in zip(chains, state):
             prompt_out[n] = last
 
     load_ps.wait()
@@ -306,6 +312,7 @@
     for i in range(PH // 2, PH):
         inside(i)
     scan(1)
+    scan(2)
 
     for copy in (load_ds, load_hg):
         copy.wait()
@@ -331,7 +338,7 @@
                 out = out + jnp.where(row == r, from_state, 0.0)
                 n = (each * half + r) * HEADS + h
                 tt[n : n + 1, :] = eg[r : r + 1]
-            nrm[half, h // 2, RP:, (h % 2) * DV : (h % 2 + 1) * DV] = normed(out, h)
+            nrm[half, h, RP:] = normed(out, h)
     columns = tt[...].T
     for half in range(2):
         for h in range(HEADS):
@@ -342,48 +349,49 @@
                 n = token * HEADS + h
                 dec_new[token, h] = columns[:, n : n + 1] * ds[token, h] + fresh
 
+    peers_out = (peer0, peer1, peer)
+
     def nrm_copy(s):
+        heads = STAGES[s]
         return pltpu.make_async_remote_copy(
-            src_ref=nrm.at[other, s], dst_ref=peer0 if s == 0 else peer, send_sem=nrm_sem.at[s], recv_sem=nrm_sem.at[2 + s],
-            device_id={"tp": other}, device_id_type=MESH,
+            src_ref=nrm.at[other, heads[0] : heads[-1] + 1], dst_ref=peers_out[s],
+            send_sem=nrm_sem.at[0, s], recv_sem=nrm_sem.at[1, s], device_id={"tp": other}, device_id_type=MESH,
         )
 
     tile = 256
-    for s in range(2):
-        for frm in peers:
-            back_copy(s, frm, frm).wait_recv()
-        for p in range(PR):
-            for e in range(2):
-                m = p * 2 + e
-                incoming = inc[s, :, m].astype(F32).reshape(DK, DV).astype(BF16)
+    for s, heads in enumerate(STAGES):
+        wait_all(inc[s], in_sem.at[1, s])
+        for e, h in enumerate(heads):
+            for p in range(PR):
+                incoming = inc[s][:, e * PR + p].astype(F32).reshape(DK, DV).astype(BF16)
                 for half in range(2):
-                    out = att[4 * s + m, half] + dot(sqc[4 * s + m, half], incoming)
-                    nrm[half, s, p * OWN : (p + 1) * OWN, e * DV : (e + 1) * DV] = normed(out, 2 * s + e)
+                    out = att[h * PR + p, half] + dot(sqc[h * PR + p, half], incoming)
+                    nrm[half, h, p * OWN : (p + 1) * OWN] = normed(out, h)
         nrm_copy(s).start()
-        left = in_position_order(order, nrm[tp, s])
-        out_loads[s].wait()
-        if s == 0:
+        if s == 1:
+            left = in_position_order(order, [nrm[tp, h] for h in range(3)])
+            out_loads[0].wait()
             for n in range(width // tile):
                 cols = slice(n * tile, (n + 1) * tile)
-                acc[:, cols] = dot(left, wo[:quarter, cols])
-        else:
-            out_loads[2].wait()
-            nrm_copy(0).wait()
-            left = jnp.concatenate([left, in_position_order(order, peer0[...])], axis=1)
-            for n in range(width // tile):
-                cols = slice(n * tile, (n + 1) * tile)
-                acc[:, cols] += dot(left, wo[quarter:, cols])
-    nrm_copy(1).wait()
-    out_loads[3].wait()
-    for to in peers:
-        total_copy(to, kv).wait_send()
-        for s in range(2):
-            state_copy(s, to, kv).wait_send()
-            back_copy(s, to, kv).wait_send()
-
-
-def in_position_order(order, part):
-    return jnp.concatenate([dotg(order, part[:RP], TN).astype(BF16), part[RP:]], axis=0)
+                acc[:, cols] = dot(left, wo[: 3 * DV, cols])
+    out_loads[1].wait()
+    for s in range(2):
+        nrm_copy(s).wait()
+    left = in_position_order(order, [nrm[tp, 3], peer0[0], peer1[0], peer1[1]])
+    for n in range(width // tile):
+        cols = slice(n * tile, (n + 1) * tile)
+        acc[:, cols] += dot(left, wo[3 * DV :, cols])
+    nrm_copy(2).wait()
+    out_loads[2].wait()
+    wait_all(ttt, tt_sem.at[0])
+    for s in range(len(STAGES)):
+        wait_all(st[s], st_sem.at[0, s])
+        wait_all(sb[s], in_sem.at[0, s])
+
+
+def in_position_order(order, parts):
+    cut = [jnp.concatenate([dotg(order, part[:RP], TN).astype(BF16), part[RP:]], axis=0) for part in parts]
+    return jnp.concatenate(cut, axis=1)
 
 
 def finish_kernel(acc, peer, w_last, prompt_in, dec_in, mixed, mixed_dec, prompt_out, dec_out, out3, out2, sem, tile_sem):
@@ -392,7 +400,7 @@
     for copy in copies:
         copy.start()
     order = order_matrix()
-    left = in_position_order(order, peer[...])
+    left = in_position_order(order, [peer[0]])
     tile = 256
 
     def out_copy(n):
@@ -427,8 +435,8 @@
         name="attend",
         out_shape=(
             jax.ShapeDtypeStruct((ROWS, width), F32),
-            jax.ShapeDtypeStruct((ROWS, 2 * DV), BF16),
-            jax.ShapeDtypeStruct((width // 4, width), BF16),
+            jax.ShapeDtypeStruct((1, ROWS, DV), BF16),
+            jax.ShapeDtypeStruct((DV, width), BF16),
             jax.ShapeDtypeStruct((PH, ROW_K, DV), F32),
             jax.ShapeDtypeStruct((4, HEADS, DK, DV), F32),
         ),
@@ -446,7 +454,7 @@
             pltpu.VMEM((1, width), F32),
             pltpu.VMEM((PH, ROW_K, DV), F32),
             pltpu.VMEM((4, HEADS, DK, DV), F32),
-            pltpu.VMEM((3 * width // 4, width), BF16),
+            pltpu.VMEM((7 * DV, width), BF16),
             pltpu.VMEM((RP, width), F32),
             pltpu.VMEM((2, ROWS, width), BF16),
             pltpu.VMEM((HEADS, 2, ROWS, DK), BF16),
@@ -454,27 +462,21 @@
             pltpu.VMEM((HEADS, 2, ROWS, DV), BF16),
             pltpu.VMEM((HEADS, 2, ROWS, DK), F32),
             pltpu.VMEM((HEADS, 2, PR, OWN, DK), F32),
-            pltpu.VMEM((2, KVN, 4, ROW_K, DV), BF16),
             pltpu.VMEM((DK, DK), F32),
             pltpu.VMEM((KVN, ROW_K, DK), F32),
-            pltpu.VMEM((2, KVN, 4, ROW_K, DV), BF16),
             pltpu.VMEM((KVN, ROW_K, DK), F32),
-            pltpu.VMEM((2, KVN, 4, ROW_K, DV), BF16),
-            pltpu.VMEM((2, KVN, 4, ROW_K, DV), BF16),
+            *(pltpu.VMEM((KVN, PR * len(heads), ROW_K, DV), BF16) for _ in range(4) for heads in STAGES),
+            *(pltpu.VMEM((len(heads), ROWS, DV), BF16) for heads in STAGES[:2]),
             pltpu.VMEM((PH, 2, OWN, DV), F32),
             pltpu.VMEM((PH, 2, OWN, DK), BF16),
-            pltpu.VMEM((2, 2, ROWS, 2 * DV), BF16),
-            pltpu.VMEM((ROWS, 2 * DV), BF16),
+            pltpu.VMEM((2, HEADS, ROWS, DV), BF16),
             dma((11,)),
-            dma((4,)),
+            dma((3,)),
             dma((2,)),
-            dma((2, KVN)),
-            dma((2, KVN)),
-            dma((KVN,)),
-            dma((KVN,)),
-            dma((2, KVN)),
-            dma((2, KVN)),
-            dma((4,)),
+            dma((2, len(STAGES))),
+            dma((2,)),
+            dma((2, len(STAGES))),
+            dma((2, len(STAGES))),
         ],
         compiler_params=pltpu.CompilerParams(collective_id=0, has_side_effects=True, vmem_limit_bytes=40 * 1024 * 1024),
     )(

time: 35.7 us -> 33.4 us (0.936)
  Pallas kernels: 34.8 us -> 32.5 us
    pallas_call x1, Pallas kernels: 32.4 us -> 30.7 us  [on_device(): pl.pallas_call(attend_kernel, name='attend', out_shape=(jax.ShapeDtypeStr...]
    pallas_call x1, Pallas kernels: 2.4 us -> 1.78 us  [on_device(): pl.pallas_call(finish_kernel, name='finish', out_shape=(jax.ShapeDtypeStr...]
where the time goes in v6:
time: 33.4 us; the launch traced here: 33.3 us
  Pallas kernels  32.5 us (97%)
  between operations  0.8 us (2%)
    pallas_call x1, Pallas kernels, on_device(): pl.pallas_call(attend_kernel, name='attend', out_shape=(jax.ShapeDtypeStr...  30.7 us
    pallas_call x1, Pallas kernels, on_device(): pl.pallas_call(finish_kernel, name='finish', out_shape=(jax.ShapeDtypeStr...  1.78 us

profile of v6, /device:TPU:1, one launch (start us, length us, event | category | flops | bytes accessed | tf_op | source)
XLA Modules:
  0.0 33.3 jit_solution(16163576855021345273)
XLA Ops:
  0.6 30.7 %attend.1 = (f32[272,2048]{1,0:T(8,128)S(1)}, bf16[1,272,256]{2,1,0:T(8,128)(2,1)S(1)}, bf16[256,2048]{1,0:T(8,128)(2,1)S(1)}, f32[8,8,256]{2,1,0:T(8,128)S(1)}, f32[4,4,128,256]{3,2,1,0:T(8,128)S(1)}) custom-call(bf16[128,2,2048]{2,1,0:T(2,128)(2,1)} %pieces.1, bf16[2,2048]{1,0:T(2,128)(2,1)} %new_tokens.1, bf16[2048,512]{1,0:T(8,128)(2,1)} %w_query.1, ...), custom_call_target="tpu_custom_call" | custom-call | tf_op jit(solution)/shard_map/attend/pallas_call | solution.py:433
  31.4 1.8 %finish.1 = (bf16[128,2,2048]{2,1,0:T(2,128)(2,1)}, bf16[2,2048]{1,0:T(2,128)(2,1)}, f32[8,8,256]{2,1,0:T(8,128)}, f32[4,4,128,256]{3,2,1,0:T(8,128)}) custom-call(f32[272,2048]{1,0:T(8,128)S(1)} %get-tuple-element.13.acc, bf16[1,272,256]{2,1,0:T(8,128)(2,1)S(1)} %get-tuple-element.14.peer, bf16[256,2048]{1,0:T(8,128)(2,1)S(1)} %get-tuple-element.15.w_last, ...), custom_call_target="tpu_custom_call" | custom-call | tf_op jit(solution)/shard_map/finish/pallas_call | solution.py:491

commit v7 on v6

--- a/solution.py
+++ b/solution.py
@@ -83,7 +83,7 @@
     load_ps = load(8, prompt_state, ps)
     load_ds = load(9, decode_state, ds)
     load_hg = load(10, head_gain, hg_v)
-    for copy in (load_x, load_nt, load_gain, load_bias, load_d):
+    for copy in (load_x, load_nt, load_gain, load_bias, load_d, load_k):
         copy.start()
 
     barrier = pltpu.get_barrier_semaphore()
@@ -96,7 +96,7 @@
     order = order_matrix()
     for copy in (load_x, load_nt, load_gain):
         copy.wait()
-    for copy in (load_k, load_v, load_q):
+    for copy in (load_v,):
         copy.start()
     flat = x3[...].reshape(RP, width)
     step = 512
@@ -142,7 +142,7 @@
         device_id={"tp": other}, device_id_type=MESH,
     )
     row_copy.start()
-    for copy in (load_ds, load_ps, load_hg):
+    for copy in (load_q, load_ds, load_ps, load_hg):
         copy.start()
 
     load_k.wait()
@@ -200,10 +200,12 @@
     rt[kv] = ttt[kv]
 
     for s, heads in enumerate(STAGES):
-        for h in heads:
-            if h in (0, 2):
-                project(other, wk, kb, "k", h // 2, 1)
-            project(other, wv, vb, "v", h, 1)
+        if s == 0:
+            project(other, wk, kb, "k", 0, 1)
+            project(other, wv, vb, "v", 0, 1)
+        elif s == 1:
+            project(other, wk, kb, "k", 1, 1)
+            project(other, wv, vb, "v", 1, 3)
         for e, h in enumerate(heads):
             for p in range(PR):
                 at = slice(p * OWN, (p + 1) * OWN)
@@ -222,12 +224,12 @@
     quarter = width // 4
 
     def out_load(i):
-        owner, first, count = ((tp, 0, 4), (other, 0, 3), (other, 3, 1))[i]
+        owner, first, count = ((tp, 0, 1), (other, 0, 1), (tp, 1, 3), (other, 1, 2), (other, 3, 1))[i]
         src = w_out.at[pl.ds(pl.multiple_of(owner * (2 * quarter) + first * DV, DV), count * DV)]
-        dst = w_last if i == 2 else wo.at[pl.ds(4 * DV * i, count * DV)]
+        dst = w_last if i == 4 else wo.at[pl.ds((0, 1, 2, 5)[i] * DV, count * DV)]
         return pltpu.make_async_copy(src, dst, wo_sem.at[i])
 
-    out_loads = [out_load(i) for i in range(3)]
+    out_loads = [out_load(i) for i in range(5)]
     for copy in out_loads:
         copy.start()
     load_q.wait()
@@ -368,21 +370,23 @@
                     out = att[h * PR + p, half] + dot(sqc[h * PR + p, half], incoming)
                     nrm[half, h, p * OWN : (p + 1) * OWN] = normed(out, h)
         nrm_copy(s).start()
-        if s == 1:
-            left = in_position_order(order, [nrm[tp, h] for h in range(3)])
-            out_loads[0].wait()
-            for n in range(width // tile):
-                cols = slice(n * tile, (n + 1) * tile)
-                acc[:, cols] = dot(left, wo[: 3 * DV, cols])
-    out_loads[1].wait()
-    for s in range(2):
-        nrm_copy(s).wait()
-    left = in_position_order(order, [nrm[tp, 3], peer0[0], peer1[0], peer1[1]])
-    for n in range(width // tile):
-        cols = slice(n * tile, (n + 1) * tile)
-        acc[:, cols] += dot(left, wo[3 * DV :, cols])
+        if s == 0:
+            nrm_copy(0).wait()
+            parts, at = [nrm[tp, 0], peer0[0]], 0
+        elif s == 1:
+            parts, at = [nrm[tp, 1], nrm[tp, 2]], 2
+        else:
+            nrm_copy(1).wait()
+            parts, at = [nrm[tp, 3], peer1[0], peer1[1]], 4
+        for i in ((0, 1), (2,), (3,))[s]:
+            out_loads[i].wait()
+        left = in_position_order(order, parts)
+        for n in range(width // tile):
+            cols = slice(n * tile, (n + 1) * tile)
+            got = dot(left, wo[at * DV : (at + len(parts)) * DV, cols])
+            acc[:, cols] = acc[:, cols] + got if s else got
     nrm_copy(2).wait()
-    out_loads[2].wait()
+    out_loads[4].wait()
     wait_all(ttt, tt_sem.at[0])
     for s in range(len(STAGES)):
         wait_all(st[s], st_sem.at[0, s])
@@ -471,7 +475,7 @@
             pltpu.VMEM((PH, 2, OWN, DK), BF16),
             pltpu.VMEM((2, HEADS, ROWS, DV), BF16),
             dma((11,)),
-            dma((3,)),
+            dma((5,)),
             dma((2,)),
             dma((2, len(STAGES))),
             dma((2,)),

time: 33.4 us -> 33.2 us (level)
  no operation moved by 1% of the time
where the time goes in v7:
time: 33.2 us; the launch traced here: 33.1 us
  Pallas kernels  32.3 us (97%)
  between operations  0.8 us (2%)
    pallas_call x1, Pallas kernels, on_device(): pl.pallas_call(attend_kernel, name='attend', out_shape=(jax.ShapeDtypeStr...  30.6 us
    pallas_call x1, Pallas kernels, on_device(): pl.pallas_call(finish_kernel, name='finish', out_shape=(jax.ShapeDtypeStr...  1.78 us

profile of v7, /device:TPU:1, one launch (start us, length us, event | category | flops | bytes accessed | tf_op | source)
XLA Modules:
  0.0 33.1 jit_solution(17122809730422524055)
XLA Ops:
  0.6 30.6 %attend.1 = (f32[272,2048]{1,0:T(8,128)S(1)}, bf16[1,272,256]{2,1,0:T(8,128)(2,1)S(1)}, bf16[256,2048]{1,0:T(8,128)(2,1)S(1)}, f32[8,8,256]{2,1,0:T(8,128)S(1)}, f32[4,4,128,256]{3,2,1,0:T(8,128)S(1)}) custom-call(bf16[128,2,2048]{2,1,0:T(2,128)(2,1)} %pieces.1, bf16[2,2048]{1,0:T(2,128)(2,1)} %new_tokens.1, bf16[2048,512]{1,0:T(8,128)(2,1)} %w_query.1, ...), custom_call_target="tpu_custom_call" | custom-call | tf_op jit(solution)/shard_map/attend/pallas_call | solution.py:437
  31.2 1.8 %finish.1 = (bf16[128,2,2048]{2,1,0:T(2,128)(2,1)}, bf16[2,2048]{1,0:T(2,128)(2,1)}, f32[8,8,256]{2,1,0:T(8,128)}, f32[4,4,128,256]{3,2,1,0:T(8,128)}) custom-call(f32[272,2048]{1,0:T(8,128)S(1)} %get-tuple-element.13.acc, bf16[1,272,256]{2,1,0:T(8,128)(2,1)S(1)} %get-tuple-element.14.peer, bf16[256,2048]{1,0:T(8,128)(2,1)S(1)} %get-tuple-element.15.w_last, ...), custom_call_target="tpu_custom_call" | custom-call | tf_op jit(solution)/shard_map/finish/pallas_call | solution.py:495

commit v8 on v7

--- a/solution.py
+++ b/solution.py
@@ -314,7 +314,6 @@
     for i in range(PH // 2, PH):
         inside(i)
     scan(1)
-    scan(2)
 
     for copy in (load_ds, load_hg):
         copy.wait()
@@ -351,6 +350,7 @@
                 n = token * HEADS + h
                 dec_new[token, h] = columns[:, n : n + 1] * ds[token, h] + fresh
 
+    scan(2)
     peers_out = (peer0, peer1, peer)
 
     def nrm_copy(s):

time: 33.2 us -> 33.2 us (level)
  no operation moved by 1% of the time
where the time goes in v8:
time: 33.2 us; the launch traced here: 33.1 us
  Pallas kernels  32.3 us (97%)
  between operations  0.8 us (2%)
    pallas_call x1, Pallas kernels, on_device(): pl.pallas_call(attend_kernel, name='attend', out_shape=(jax.ShapeDtypeStr...  30.6 us
    pallas_call x1, Pallas kernels, on_device(): pl.pallas_call(finish_kernel, name='finish', out_shape=(jax.ShapeDtypeStr...  1.78 us

profile of v8, /device:TPU:1, one launch (start us, length us, event | category | flops | bytes accessed | tf_op | source)
XLA Modules:
  0.0 33.1 jit_solution(12874339722850676610)
XLA Ops:
  0.6 30.6 %attend.1 = (f32[272,2048]{1,0:T(8,128)S(1)}, bf16[1,272,256]{2,1,0:T(8,128)(2,1)S(1)}, bf16[256,2048]{1,0:T(8,128)(2,1)S(1)}, f32[8,8,256]{2,1,0:T(8,128)S(1)}, f32[4,4,128,256]{3,2,1,0:T(8,128)S(1)}) custom-call(bf16[128,2,2048]{2,1,0:T(2,128)(2,1)} %pieces.1, bf16[2,2048]{1,0:T(2,128)(2,1)} %new_tokens.1, bf16[2048,512]{1,0:T(8,128)(2,1)} %w_query.1, ...), custom_call_target="tpu_custom_call" | custom-call | tf_op jit(solution)/shard_map/attend/pallas_call | solution.py:437
  31.2 1.8 %finish.1 = (bf16[128,2,2048]{2,1,0:T(2,128)(2,1)}, bf16[2,2048]{1,0:T(2,128)(2,1)}, f32[8,8,256]{2,1,0:T(8,128)}, f32[4,4,128,256]{3,2,1,0:T(8,128)}) custom-call(f32[272,2048]{1,0:T(8,128)S(1)} %get-tuple-element.13.acc, bf16[1,272,256]{2,1,0:T(8,128)(2,1)S(1)} %get-tuple-element.14.peer, bf16[256,2048]{1,0:T(8,128)(2,1)S(1)} %get-tuple-element.15.w_last, ...), custom_call_target="tpu_custom_call" | custom-call | tf_op jit(solution)/shard_map/finish/pallas_call | solution.py:495
